TPU v7x, 32 devices: a whole 2x2x4 slice. The times are simulated.
32 devices in a mesh: sp: 4 (over y, x), tp: 8 (over z, core).
Axes of the slice: x: 2, y: 2, z: 4, core: 2. Of those that a mesh axis runs over, the one named last changes fastest.
Arguments:
- conv_in: bfloat16 [1024, 16384], P('tp', 'sp'), may hold values from -6 to 6
- in_gate: bfloat16 [1024, 16384], P('tp', 'sp'), may hold values from -6 to 6
- out_gate: bfloat16 [1024, 16384], P('tp', 'sp'), may hold values from -6 to 6
- doc_ids: int32 [16384], P('sp'), may hold values from 0 to 1, never falling along the last dimension, each value on 1 to 12288 neighbouring positions
- conv_taps: float32 [1024, 3], P('tp'), may hold values from -3.5 to 3.5
- head_gain: float32 [1024], P('tp'), may hold values from 0.1 to 1.9
- out_proj: bfloat16 [1024, 2048], P('tp'), may hold values from -0.1875 to 0.1875
- resid: bfloat16 [16384, 2048], P(('sp', 'tp')), may hold values from -6 to 6
- norm_gain: float32 [2048], replicated, may hold values from 0.1 to 1.9
- route_ids: int32 [16384, 2], P(('sp', 'tp')), may hold values from 0 to 15, all different within a row; in each aligned block of 256 rows (0 to 255, 256 to 511, ...) at most 64 rows name the same one
- route_weight: float32 [16384, 2], P(('sp', 'tp')), may hold values from 0.1 to 1
- w_gate: bfloat16 [16, 2048, 512], P('sp'), may hold values from -0.125 to 0.125
- w_up: bfloat16 [16, 2048, 512], P('sp'), may hold values from -0.125 to 0.125
- w_down: bfloat16 [16, 512, 2048], P('sp'), may hold values from -0.25 to 0.25
Outputs:
- layer_out: bfloat16 [16384, 2048], P(('sp', 'tp'))
Inputs may be any that keep to these rules, and one draw needn't show every extreme that they name: `doc_ids`: document numbers never fall along the sequence; every number from 0 to 1 is used; no document is longer than 12288 positions and one is exactly that long. `route_ids`: each position names 2 different experts. In every aligned block of 256 positions no expert is named by more than 64 positions, a bound that some block reaches.
All inputs are finite; a program needn't handle non-finite values.
Results may differ from a plain program's by a relative error of at most 0.0051.
Values may be sent and summed in bfloat16 or wider, within the bound.
A program may use at most 128 MiB of HBM per device.

v0:
```python
import jax
import jax.numpy as jnp
from jax import lax
from jax.sharding import PartitionSpec as P

HEAD = 64


norm_eps = 1e-06


def shifted(value, axis, steps):
    count = lax.axis_size(axis)
    leading, last = (max(0, -steps), min(count, count - steps))
    return lax.ppermute(value, axis, [(source, source + steps) for source in range(leading, last)])


def slot_places(ids_block, slot, experts):
    flat = ids_block.reshape(-1)
    marks = (flat[:, None] == jnp.arange(experts, dtype=jnp.int32)[None, :]).astype(jnp.int32)
    before = jnp.sum((jnp.cumsum(marks, axis=0) - 1) * marks, axis=1)
    return (flat * slot + before).reshape(ids_block.shape)


def pack_rows(places, normed_rows, total_slots):
    targets = jnp.arange(total_slots, dtype=jnp.int32)
    table = jnp.any(targets[:, None, None] == places[None, :, :], axis=2).astype(jnp.bfloat16)
    return jnp.dot(table, normed_rows, preferred_element_type=jnp.float32).astype(jnp.bfloat16)


def combine_rows(returned, places, weights):
    totals = jnp.zeros((places.shape[0], returned.shape[1]), jnp.float32)
    for choice_k in range(places.shape[1]):
        totals = totals + weights[:, choice_k : choice_k + 1] * returned[
            places[:, choice_k]
        ].astype(jnp.float32)
    return totals


def neighbour(value, bit):
    count = lax.axis_size("sp")
    return lax.ppermute(value, "sp", [(source, source ^ bit) for source in range(count)])


def gather_near(value):
    return value, neighbour(value, 1), neighbour(value, 2)


def gather_far(value, from_one, from_two):
    middle = value.shape[0] // 2
    low = neighbour(from_one[:middle], 2)
    high = neighbour(from_two[middle:], 1)
    return [value, from_one, from_two, jnp.concatenate([low, high], axis=0)]


def scatter_four(parts):
    middle = parts[3].shape[0] // 2
    low = neighbour(parts[3][:middle], 1)
    high = neighbour(parts[3][middle:], 2)
    straight = neighbour(parts[1][:middle], 1), neighbour(parts[2][middle:], 2)
    return straight, (add(parts[1][middle:], high), add(parts[2][:middle], low))


def scatter_rest(straight, joined):
    one = jnp.concatenate([straight[0], neighbour(joined[0], 1)], axis=0)
    two = jnp.concatenate([neighbour(joined[1], 2), straight[1]], axis=0)
    return one, two


def add(left, right):
    return (left.astype(jnp.float32) + right.astype(jnp.float32)).astype(jnp.bfloat16)


def every_column(out_proj):
    me, tp_count = lax.axis_index("sp"), lax.axis_size("tp")
    rows, width = out_proj.shape
    mine = lax.dynamic_slice_in_dim(out_proj, me * (width // 4), width // 4, axis=1)
    mine = jnp.transpose(mine.reshape(rows, 2, width // 8), (1, 0, 2))
    mine = jnp.tile(mine, (tp_count // 2, 1, 1))
    mine = lax.all_to_all(mine, "tp", split_axis=0, concat_axis=0, tiled=True)
    return mine.reshape(tp_count * rows, width // 8)


def other_core(value):
    count = lax.axis_size("tp")
    return lax.ppermute(value, "tp", [(source, source ^ 1) for source in range(count)])


def mix(by_row, mine):
    parts = []
    for part in gather_far(*gather_near(mine)):
        parts.extend([part, other_core(part)])
    stacked = jnp.stack(parts)
    me, core = lax.axis_index("sp"), lax.axis_index("tp") % 2
    order = [
        stacked[2 * (me ^ column) + (core ^ parity)] for column in range(4) for parity in range(2)
    ]
    return lax.dot_general(
        by_row,
        jnp.concatenate(order, axis=1),
        (((0,), (0,)), ((), ())),
        preferred_element_type=jnp.float32,
    )


def route_lists(route_ids, route_weight):
    listing = jnp.concatenate([route_ids.astype(jnp.float32), route_weight], axis=1).T
    return jnp.stack([listing] + [neighbour(listing, distance) for distance in range(1, 4)])


def route_tables(everyone, local_experts, half, slot):
    me = lax.axis_index("sp")
    top = everyone.shape[1] // 2
    ids = everyone[:, :top].astype(jnp.int32).reshape(4, top, -1, half)
    weights = everyone[:, top:].reshape(4, top, -1, half)
    experts = me * local_experts + jnp.arange(local_experts, dtype=jnp.int32)
    hit = ids[:, :, :, None, :] == experts[None, None, None, :, None]
    marks = jnp.any(hit, axis=1)
    weight_of = jnp.sum(jnp.where(hit, weights[:, :, :, None], 0.0), axis=1)
    earlier = (
        jnp.arange(half)[:, None] < jnp.arange(half)[None, :]
    ).astype(jnp.bfloat16)
    rank = jnp.dot(
        marks.astype(jnp.bfloat16).reshape(-1, half), earlier, preferred_element_type=jnp.float32
    ).reshape(marks.shape)
    rank = jnp.where(marks, rank.astype(jnp.int32), -1)
    chosen = rank[:, :, :, None, :] == jnp.arange(slot, dtype=jnp.int32)[None, None, None, :, None]
    slot_weight = jnp.sum(jnp.where(chosen, weight_of[:, :, :, None, :], 0.0), axis=4)
    return chosen.astype(jnp.bfloat16), slot_weight


def experts_on(rows, table, slot_weight, w_gate, w_up, w_down, held, late):
    sources, local_experts, slot, half = table.shape
    width = rows.shape[2]
    packed = jnp.einsum("nest,ntd->ensd", table, rows, preferred_element_type=jnp.float32)
    packed = packed.astype(jnp.bfloat16).reshape(local_experts, sources * slot, width)
    gate_part = jnp.einsum("emd,edf->emf", packed, w_gate, preferred_element_type=jnp.float32)
    up_part = jnp.einsum("emd,edf->emf", packed, w_up, preferred_element_type=jnp.float32)
    hidden = (jax.nn.silu(gate_part) * up_part).astype(jnp.bfloat16)
    if late:
        hidden = lax.optimization_barrier(hidden)
    else:
        hidden, held = lax.optimization_barrier((hidden, held))
    down = jnp.einsum("emf,efd->emd", hidden, w_down, preferred_element_type=jnp.float32)
    scale = jnp.transpose(slot_weight, (1, 0, 2)).reshape(local_experts, sources * slot, 1)
    down = (down * scale).astype(jnp.bfloat16).reshape(local_experts, sources, slot, width)
    if late:
        down, held = lax.optimization_barrier((down, held))
    total = jnp.einsum("nest,ensd->ntd", table, down, preferred_element_type=jnp.float32)
    return total.astype(jnp.bfloat16), held


def body(
    conv_in,
    in_gate,
    out_gate,
    doc_ids,
    conv_taps,
    head_gain,
    out_proj,
    resid,
    norm_gain,
    route_ids,
    route_weight,
    w_gate,
    w_up,
    w_down,
):
    gated_in = in_gate.astype(jnp.float32) * conv_in.astype(jnp.float32)
    doc_value = doc_ids.astype(jnp.float32)
    edge = jnp.concatenate([gated_in[:, -2:], doc_value[None, -2:]], axis=0)
    edge = shifted(edge, "sp", 1)
    earlier_in, earlier_doc = edge[:-1], edge[-1]
    padded_in = jnp.concatenate([earlier_in, gated_in], axis=1)
    padded_doc = jnp.concatenate([earlier_doc, doc_value])
    same_one = (padded_doc[1:-1] == doc_value).astype(jnp.float32)
    same_two = (padded_doc[:-2] == doc_value).astype(jnp.float32)
    conv_out = (
        conv_taps[:, 2:3] * gated_in
        + conv_taps[:, 1:2] * (padded_in[:, 1:-1] * same_one)
        + conv_taps[:, 0:1] * (padded_in[:, :-2] * same_two)
    )
    gated_out = out_gate.astype(jnp.float32) * conv_out
    channels = gated_out.shape[0]
    by_head = gated_out.reshape(channels // HEAD, HEAD, -1)
    by_head = by_head * lax.rsqrt(jnp.mean(by_head * by_head, axis=1, keepdims=True) + norm_eps)
    head_normed = (by_head.reshape(channels, -1) * head_gain[:, None]).astype(jnp.bfloat16)
    rows = resid.shape[0]
    width = resid.shape[1]
    half = rows // 2
    slot = max(2, rows // 8)
    sp_count = lax.axis_size("sp")
    local_experts = w_gate.shape[0]
    whole_rows = (
        sp_count == 4
        and lax.axis_size("tp") % 2 == 0
        and width % 1024 == 0
        and rows <= 2 * local_experts * slot
    )
    if whole_rows:
        mine, everyone = every_column(out_proj), route_lists(route_ids, route_weight)
        head_normed, mine, everyone = lax.optimization_barrier((head_normed, mine, everyone))
    by_row = lax.all_to_all(head_normed, "tp", split_axis=1, concat_axis=0, tiled=True)
    if whole_rows:
        tables, slot_weights = route_tables(everyone, local_experts, half, slot)
        by_row, tables, slot_weights = lax.optimization_barrier((by_row, tables, slot_weights))
        mixed = mix(by_row, mine)
    else:
        mixed = lax.dot_general(
            by_row,
            lax.all_gather(out_proj, "tp", axis=0, tiled=True),
            (((0,), (0,)), ((), ())),
            preferred_element_type=jnp.float32,
        )
    stream = resid.astype(jnp.float32) + mixed
    expert_in = (
        stream * lax.rsqrt(jnp.mean(stream * stream, axis=1, keepdims=True) + norm_eps) * norm_gain
    ).astype(jnp.bfloat16)
    experts_total = local_experts * sp_count
    if whole_rows:
        near = gather_near(expert_in[:half])
        later, near = lax.optimization_barrier((expert_in[half:], near))
        held = gather_near(later)
        rows_of = jnp.stack(gather_far(*near))
        partials, sent = [], []
        for block_no in range(2):
            partial, held = experts_on(
                rows_of,
                tables[:, block_no],
                slot_weights[:, block_no],
                w_gate,
                w_up,
                w_down,
                held,
                block_no > 0,
            )
            if block_no == 0:
                rows_of = jnp.stack(gather_far(*held))
            else:
                sent.append(scatter_rest(*held))
            partials.append(partial[0])
            held = scatter_four([partial[distance] for distance in range(4)])
        sent.append(scatter_rest(*held))
        totals = []
        for block_no in range(2):
            one, two = sent[block_no]
            own = stream[block_no * half : (block_no + 1) * half]
            own = own + partials[block_no].astype(jnp.float32)
            totals.append(own + one.astype(jnp.float32) + two.astype(jnp.float32))
        return jnp.concatenate(totals, axis=0).astype(jnp.bfloat16)
    parts = []
    for block_no in range(2):
        block_ids = route_ids[block_no * half : (block_no + 1) * half]
        place = slot_places(block_ids, slot, experts_total)
        send = pack_rows(
            place, expert_in[block_no * half : (block_no + 1) * half], experts_total * slot
        ).reshape(sp_count, local_experts, slot, width)
        arrived = lax.all_to_all(send, "sp", split_axis=0, concat_axis=0, tiled=True)
        gate_part = jnp.einsum(
            "nesd,edf->nesf", arrived, w_gate, preferred_element_type=jnp.float32
        )
        up_part = jnp.einsum("nesd,edf->nesf", arrived, w_up, preferred_element_type=jnp.float32)
        hidden = (jax.nn.silu(gate_part) * up_part).astype(jnp.bfloat16)
        arrived = jnp.einsum(
            "nesf,efd->nesd", hidden, w_down, preferred_element_type=jnp.float32
        ).astype(jnp.bfloat16)
        returned = lax.all_to_all(arrived, "sp", split_axis=0, concat_axis=0, tiled=True).reshape(
            experts_total * slot, width
        )
        parts.append(
            combine_rows(returned, place, route_weight[block_no * half : (block_no + 1) * half])
        )
    mixture = jnp.concatenate(parts, axis=0)
    return (stream + mixture).astype(jnp.bfloat16)


def solution(mesh):
    return jax.shard_map(
        body,
        mesh=mesh,
        in_specs=(
            P("tp", "sp"),
            P("tp", "sp"),
            P("tp", "sp"),
            P("sp"),
            P("tp", None),
            P("tp"),
            P("tp", None),
            P(("sp", "tp"), None),
            P(),
            P(("sp", "tp"), None),
            P(("sp", "tp"), None),
            P("sp", None, None),
            P("sp", None, None),
            P("sp", None, None),
        ),
        out_specs=P(("sp", "tp"), None),
        check_vma=False,
    )
```

profile of v0, /device:TPU:8, one launch (start us, length us, event | category | flops | bytes accessed | tf_op | source)
XLA Modules:
  0.0 214.0 jit_solution(10924674135254812387)
XLA Ops:
  0.0 0.7 convert_element_type.152
  0.8 0.7 fusion.54
  1.4 1.5 collective-permute-start.2
  3.0 1.5 collective-permute-start.1
  5.2 0.8 tile.4
  6.0 5.3 %all-to-all-start = ((bf16[8,128,256]{2,1,0:T(8,128)(2,1)}), bf16[8,128,256]{2,1,0:T(8,128)(2,1)S(1)}, u32[]{:S(2)}, u32[]{:S(2)}) async-start(bf16[8,128,256]{2,1,0:T(8,128)(2,1)} %bitcast.9), calls=%async_computation | async-start | bytes 1048576 | tf_op jit(solution)/shard_map/all_to_all | solution.py:80
  11.4 0.7 convert_element_type.148
  12.2 1.8 convert_multiply_fusion
  14.1 3.4 %collective-permute-start = (f32[129,2]{1,0:T(8,128)S(1)}, f32[129,2]{1,0:T(8,128)S(1)}, u32[]{:S(2)}, u32[]{:S(2)}) collective-permute-start(f32[129,2]{1,0:T(8,128)S(1)} %pad_maximum_fusion.2), channel_id=1, source_target_pairs={{0,8},{8,16},{16,24},{1,9},{9,17},{17,25},{2,10},{10,18},{18,26},{... | collective-permute-start | bytes 3104 | tf_op jit(solution)/shard_map/ppermute | solution.py:15
  17.6 1.8 collective-permute-done
  19.5 2.5 %bitcast_reduce_fusion = (f32[2,4096]{1,0:T(2,128)S(1)}, f32[128,4096]{1,0:T(8,128)S(1)}) fusion(f32[4096]{0:T(1024)S(1)} %get-tuple-element.64, f32[128,4096]{1,0:T(8,128)S(1)} %convert_multiply_fusion, f32[128,2]{1,0:T(8,128)S(1)} %slice.220, f32[128]{0:T(128)S(1)} %get-tuple-element.70, f32[4096]{0:T(1024)S(1)} %get-tuple-element.63, ...), kind=kLoop, calls=%fused_computation.50 | loop fusion | flops 6807552 | bytes 5310976 | tf_op jit(solution)/shard_map/reduce_sum | solution.py:186
  22.5 1.0 all-to-all-done
  23.5 2.4 %collective-permute-start.7 = (bf16[1024,256]{1,0:T(8,128)(2,1)S(1)}, bf16[1024,256]{1,0:T(8,128)(2,1)S(1)}, u32[]{:S(2)}, u32[]{:S(2)}) collective-permute-start(bf16[1024,256]{1,0:T(8,128)(2,1)S(1)} %bitcast.194), channel_id=1, source_target_pairs={{0,16},{8,24},{16,0},{24,8},{1,17},{9,25},{17,1},{25,9},{2,18},{10... | collective-permute-start | bytes 1572872 | tf_op jit(solution)/shard_map/ppermute | solution.py:42
  25.8 0.6 collective-permute-start.5
  26.5 1.3 copy.74
  27.8 6.7 %all-to-all-start.1 = ((bf16[128,8,512]{0,2,1:T(8,128)(2,1)}), bf16[128,8,512]{0,2,1:T(8,128)(2,1)S(1)}, u32[]{:S(2)}, u32[]{:S(2)}) async-start(bf16[128,8,512]{0,2,1:T(8,128)(2,1)} %bitcast.16), calls=%async_computation.1 | async-start | bytes 2097152 | tf_op jit(solution)/shard_map/all_to_all | solution.py:203
  35.3 1.4 fusion.32
  37.2 1.6 collective-permute-start.10
  38.7 1.6 collective-permute-start.9
  40.9 4.8 %collective-permute-done.9 = bf16[512,256]{1,0:T(8,128)(2,1)S(1)} collective-permute-done((bf16[512,256]{1,0:T(8,128)(2,1)S(1)}, bf16[512,256]{1,0:T(8,128)(2,1)S(1)}, u32[]{:S(2)}, u32[]{:S(2)}) %collective-permute-start.9) | collective-permute-done | bytes 262176 | tf_op jit(solution)/shard_map/ppermute | solution.py:42
  46.0 1.7 collective-permute-done.11
  47.8 0.9 bitcast_dynamic-update-slice_fusion.7
  48.7 0.9 bitcast_dynamic-update-slice_fusion.6
  49.6 0.9 bitcast_dynamic-update-slice_fusion.5
  50.4 0.9 bitcast_dynamic-update-slice_fusion.4
  51.3 0.9 bitcast_dynamic-update-slice_fusion.3
  52.2 0.9 bitcast_dynamic-update-slice_fusion.2
  53.1 0.9 bitcast_dynamic-update-slice_fusion.1
  53.9 0.9 bitcast_dynamic-update-slice_fusion
  54.8 2.8 %all-to-all-done.1 = bf16[128,8,512]{0,2,1:T(8,128)(2,1)S(1)} async-done(((bf16[128,8,512]{0,2,1:T(8,128)(2,1)}), bf16[128,8,512]{0,2,1:T(8,128)(2,1)S(1)}, u32[]{:S(2)}, u32[]{:S(2)}) %all-to-all-start.1) | async-done | bytes 1048608 | tf_op jit(solution)/shard_map/all_to_all | solution.py:203
  57.6 0.7 copy.75
  58.3 5.5 %multiply_reduce_fusion = (f32[512]{0:T(512)S(1)}, f32[512,2048]{1,0:T(8,128)S(1)}) fusion(bf16[1024,512]{1,0:T(8,128)(2,1)S(1)} %bitcast.188, bf16[1024,2048]{1,0:T(8,128)(2,1)} %bitcast_dynamic-update-slice_fusion, bf16[512,2048]{1,0:T(8,128)(2,1)} %param.21), kind=kOutput, calls=%fused_computation.25 | convolution fusion | flops 2151677440 | bytes 11536384 | tf_op jit(solution)/shard_map/dot_general | solution.py:98
  64.5 1.3 copy-done.2
  67.3 23.6 %collective-permute-done.13 = bf16[256,2048]{1,0:T(8,128)(2,1)S(1)} collective-permute-done((bf16[256,2048]{1,0:T(8,128)(2,1)S(1)}, bf16[256,2048]{1,0:T(8,128)(2,1)S(1)}, u32[]{:S(2)}, u32[]{:S(2)}) %collective-permute-start.13) | collective-permute-done | bytes 1048608 | tf_op jit(solution)/shard_map/ppermute | solution.py:42
  91.0 1.0 collective-permute-done.12
  92.6 0.8 collective-permute-start.14
  93.6 1.2 collective-permute-start.17
  94.8 1.5 collective-permute-start.16
  96.3 10.7 %collective-permute-done.15 = bf16[128,2048]{1,0:T(8,128)(2,1)} collective-permute-done((bf16[128,2048]{1,0:T(8,128)(2,1)S(1)}, bf16[128,2048]{1,0:T(8,128)(2,1)}, u32[]{:S(2)}, u32[]{:S(2)}) %collective-permute-start.15) | collective-permute-done | bytes 524320 | tf_op jit(solution)/shard_map/ppermute | solution.py:42
  107.5 1.4 maximum_bitcast_fusion.8
  109.0 3.3 %convert_bitcast_fusion.1 = bf16[4,4,64,2048]{3,2,0,1:T(8,128)(2,1)S(1)} fusion(bf16[1,256,2048]{2,1,0:T(8,128)(2,1)S(1)} %maximum_bitcast_fusion.8, bf16[1,256,2048]{2,1,0:T(8,128)(2,1)} %bitcast.203, bf16[1,256,2048]{2,1,0:T(8,128)(2,1)} %bitcast.204, bf16[1,256,2048]{2,1,0:T(8,128)(2,1)} %bitcast.199, bf16[4,2,4,64,256]{4,3,2,0,1:T(8,128)(2,1)S(1)} %copy-done.4), kind=kOutput, calls=%fused_computation.23 | convolution fusion | flops 1092616192 | bytes 8912896 | tf_op jit(solution)/shard_map/nest,ntd->ensd/dot_general | solution.py:135
  112.6 2.3 %fusion.61 = f32[4,256,512]{2,1,0:T(8,128)S(1)} fusion(bf16[4,256,2048]{2,1,0:T(8,128)(2,1)S(1)} %bitcast.189, bf16[4,2048,512]{2,1,0:T(8,128)(2,1)S(1)} %bitcast.209), kind=kOutput, calls=%fused_computation.143 | convolution fusion | flops 2147483648 | bytes 14680064 | tf_op jit(solution)/shard_map/emd,edf->emf/dot_general | solution.py:137
  114.9 5.8 %multiply_convert_fusion.4 = bf16[4,256,512]{2,1,0:T(8,128)(2,1)S(1)} fusion(f32[4,256,512]{2,1,0:T(8,128)S(1)} %fusion.61, bf16[4,256,2048]{2,1,0:T(8,128)(2,1)S(1)} %bitcast.190, bf16[4,2048,512]{2,1,0:T(8,128)(2,1)} %param.26), kind=kOutput, calls=%fused_computation.52 | convolution fusion | flops 2150629376 | bytes 15728640 | tf_op jit(solution)/shard_map/emd,edf->emf/dot_general | solution.py:138
  120.8 7.1 %collective-permute-done.17 = bf16[256,2048]{1,0:T(8,128)(2,1)S(1)} collective-permute-done((bf16[256,2048]{1,0:T(8,128)(2,1)S(1)}, bf16[256,2048]{1,0:T(8,128)(2,1)S(1)}, u32[]{:S(2)}, u32[]{:S(2)}) %collective-permute-start.17) | collective-permute-done | bytes 1048608 | tf_op jit(solution)/shard_map/ppermute | solution.py:42
  127.9 1.6 collective-permute-start.19
  130.0 5.7 %multiply_convert_fusion.1 = bf16[4,256,2048]{2,1,0:T(8,128)(2,1)S(1)} fusion(bf16[4,256,512]{2,1,0:T(8,128)(2,1)S(1)} %multiply_convert_fusion.4, bf16[4,512,2048]{2,1,0:T(8,128)(2,1)} %param.27, f32[4,256]{1,0:T(4,128)S(1)} %mul.186), kind=kOutput, calls=%fused_computation.3 | convolution fusion | flops 2151677952 | bytes 13635584 | tf_op jit(solution)/shard_map/emf,efd->emd/dot_general | solution.py:144
  135.7 1.5 bitcast_convert_fusion.1
  138.1 1.5 collective-permute-start.22
  140.1 2.2 %collective-permute-done.19 = bf16[128,2048]{1,0:T(8,128)(2,1)S(1)} collective-permute-done((bf16[128,2048]{1,0:T(8,128)(2,1)S(1)}, bf16[128,2048]{1,0:T(8,128)(2,1)S(1)}, u32[]{:S(2)}, u32[]{:S(2)}) %collective-permute-start.19) | collective-permute-done | bytes 524320 | tf_op jit(solution)/shard_map/ppermute | solution.py:42
  142.4 1.9 collective-permute-start.20
  144.4 1.5 convert_bitcast_fusion
  146.2 5.9 %fusion.62 = f32[4,256,512]{2,1,0:T(8,128)S(1)} fusion(bf16[4,256,2048]{2,1,0:T(8,128)(2,1)S(1)} %bitcast.191, bf16[4,2048,512]{2,1,0:T(8,128)(2,1)} %param.25), kind=kOutput, calls=%fused_computation.144 | convolution fusion | flops 2147483648 | bytes 14680064 | tf_op jit(solution)/shard_map/emd,edf->emf/dot_general | solution.py:137
  152.1 2.5 %multiply_convert_fusion.3 = bf16[4,256,512]{2,1,0:T(8,128)(2,1)S(1)} fusion(f32[4,256,512]{2,1,0:T(8,128)S(1)} %fusion.62, bf16[4,256,2048]{2,1,0:T(8,128)(2,1)S(1)} %bitcast.192, bf16[4,2048,512]{2,1,0:T(8,128)(2,1)S(1)} %bitcast.211), kind=kOutput, calls=%fused_computation.51 | convolution fusion | flops 2150629376 | bytes 15728640 | tf_op jit(solution)/shard_map/emd,edf->emf/dot_general | solution.py:138
  154.6 5.7 %multiply_convert_fusion = bf16[4,256,2048]{2,1,0:T(8,128)(2,1)S(1)} fusion(bf16[4,256,512]{2,1,0:T(8,128)(2,1)S(1)} %multiply_convert_fusion.3, bf16[4,512,2048]{2,1,0:T(8,128)(2,1)} %param.27, f32[4,256]{1,0:T(4,128)S(1)} %mul.191), kind=kOutput, calls=%fused_computation.2 | convolution fusion | flops 2151677952 | bytes 13635584 | tf_op jit(solution)/shard_map/emf,efd->emd/dot_general | solution.py:144
  160.7 2.8 %collective-permute-done.21 = bf16[128,2048]{1,0:T(8,128)(2,1)S(1)} collective-permute-done((bf16[128,2048]{1,0:T(8,128)(2,1)S(1)}, bf16[128,2048]{1,0:T(8,128)(2,1)S(1)}, u32[]{:S(2)}, u32[]{:S(2)}) %collective-permute-start.21) | collective-permute-done | bytes 524320 | tf_op jit(solution)/shard_map/ppermute | solution.py:42
  163.6 1.3 bitcast_convert_fusion
  166.0 1.5 collective-permute-start.24
  167.5 1.7 collective-permute-start.25
  169.5 10.5 %collective-permute-done.29 = bf16[128,2048]{1,0:T(8,128)(2,1)S(1)} collective-permute-done((bf16[128,2048]{1,0:T(8,128)(2,1)S(1)}, bf16[128,2048]{1,0:T(8,128)(2,1)S(1)}, u32[]{:S(2)}, u32[]{:S(2)}) %collective-permute-start.29) | collective-permute-done | bytes 524320 | tf_op jit(solution)/shard_map/ppermute | solution.py:42
  181.3 9.9 %collective-permute-done.24 = bf16[128,2048]{1,0:T(8,128)(2,1)S(1)} collective-permute-done((bf16[128,2048]{1,0:T(8,128)(2,1)S(1)}, bf16[128,2048]{1,0:T(8,128)(2,1)S(1)}, u32[]{:S(2)}, u32[]{:S(2)}) %collective-permute-start.24) | collective-permute-done | bytes 524320 | tf_op jit(solution)/shard_map/ppermute | solution.py:42
  191.8 11.2 %collective-permute-done.31 = bf16[128,2048]{1,0:T(8,128)(2,1)S(1)} collective-permute-done((bf16[128,2048]{1,0:T(8,128)(2,1)S(1)}, bf16[128,2048]{1,0:T(8,128)(2,1)S(1)}, u32[]{:S(2)}, u32[]{:S(2)}) %collective-permute-start.31) | collective-permute-done | bytes 524320 | tf_op jit(solution)/shard_map/ppermute | solution.py:42
  203.0 7.6 %collective-permute-done.30 = bf16[128,2048]{1,0:T(8,128)(2,1)S(1)} collective-permute-done((bf16[128,2048]{1,0:T(8,128)(2,1)S(1)}, bf16[128,2048]{1,0:T(8,128)(2,1)S(1)}, u32[]{:S(2)}, u32[]{:S(2)}) %collective-permute-start.30) | collective-permute-done | bytes 524320 | tf_op jit(solution)/shard_map/ppermute | solution.py:42
  210.7 1.8 fusion.27
  212.4 1.6 pad_maximum_fusion.1
  (119 shorter events, 13.3 us)
Async XLA Ops:
  0.0 4.9 %copy-start = (bf16[128,2048]{1,0:T(8,128)(2,1)S(1)}, bf16[128,2048]{1,0:T(8,128)(2,1)}, u32[]{:S(2)}) copy-start(bf16[128,2048]{1,0:T(8,128)(2,1)} %param.20) | copy-start | bytes 1572868
  0.0 17.5 %copy-start.9 = (f32[128,3]{0,1:T(4,128)S(1)}, f32[128,3]{0,1:T(4,128)}, u32[]{:S(2)}) copy-start(f32[128,3]{0,1:T(4,128)} %param.18) | copy-start | bytes 4612
  1.4 21.0 %collective-permute-start.2 = (f32[4,512]{1,0:T(4,128)S(1)}, f32[4,512]{1,0:T(4,128)S(1)}, u32[]{:S(2)}, u32[]{:S(2)}) collective-permute-start(f32[4,512]{1,0:T(4,128)S(1)} %get-tuple-element.68), channel_id=1, source_target_pairs={{0,16},{8,24},{16,0},{24,8},{1,17},{9,25},{17,1},{25,9},{2,18},{10... | collective-permute-start | bytes 24584 | tf_op jit(solution)/shard_map/ppermute | solution.py:42
  3.0 19.5 %collective-permute-start.1 = (f32[4,512]{1,0:T(4,128)S(1)}, f32[4,512]{1,0:T(4,128)S(1)}, u32[]{:S(2)}, u32[]{:S(2)}) collective-permute-start(f32[4,512]{1,0:T(4,128)S(1)} %get-tuple-element.68), channel_id=1, source_target_pairs={{0,8},{8,0},{16,24},{24,16},{1,9},{9,1},{17,25},{25,17},{2,10},{10... | collective-permute-start | bytes 24584 | tf_op jit(solution)/shard_map/ppermute | solution.py:42
  4.5 18.0 %collective-permute-start.3 = (f32[4,512]{1,0:T(4,128)S(1)}, f32[4,512]{1,0:T(4,128)S(1)}, u32[]{:S(2)}, u32[]{:S(2)}) collective-permute-start(f32[4,512]{1,0:T(4,128)S(1)} %get-tuple-element.68), channel_id=1, source_target_pairs={{0,24},{8,16},{16,8},{24,0},{1,25},{9,17},{17,9},{25,1},{2,26},{10... | collective-permute-start | bytes 24584 | tf_op jit(solution)/shard_map/ppermute | solution.py:42
  6.0 17.4 %all-to-all-start = ((bf16[8,128,256]{2,1,0:T(8,128)(2,1)}), bf16[8,128,256]{2,1,0:T(8,128)(2,1)S(1)}, u32[]{:S(2)}, u32[]{:S(2)}) async-start(bf16[8,128,256]{2,1,0:T(8,128)(2,1)} %bitcast.9), calls=%async_computation | async-start | bytes 1048576 | tf_op jit(solution)/shard_map/all_to_all | solution.py:80
  12.1 9.9 %copy-start.10 = (f32[128]{0:T(128)S(1)}, f32[128]{0:T(128)}, u32[]{:S(2)}) copy-start(f32[128]{0:T(128)} %param.19) | copy-start | bytes 1540
  14.1 5.3 %collective-permute-start = (f32[129,2]{1,0:T(8,128)S(1)}, f32[129,2]{1,0:T(8,128)S(1)}, u32[]{:S(2)}, u32[]{:S(2)}) collective-permute-start(f32[129,2]{1,0:T(8,128)S(1)} %pad_maximum_fusion.2), channel_id=1, source_target_pairs={{0,8},{8,16},{16,24},{1,9},{9,17},{17,25},{2,10},{10,18},{18,26},{... | collective-permute-start | bytes 3104 | tf_op jit(solution)/shard_map/ppermute | solution.py:15
  23.5 13.7 %collective-permute-start.7 = (bf16[1024,256]{1,0:T(8,128)(2,1)S(1)}, bf16[1024,256]{1,0:T(8,128)(2,1)S(1)}, u32[]{:S(2)}, u32[]{:S(2)}) collective-permute-start(bf16[1024,256]{1,0:T(8,128)(2,1)S(1)} %bitcast.194), channel_id=1, source_target_pairs={{0,16},{8,24},{16,0},{24,8},{1,17},{9,25},{17,1},{25,9},{2,18},{10... | collective-permute-start | bytes 1572872 | tf_op jit(solution)/shard_map/ppermute | solution.py:42
  25.8 12.9 %collective-permute-start.5 = (bf16[1024,256]{1,0:T(8,128)(2,1)S(1)}, bf16[1024,256]{1,0:T(8,128)(2,1)S(1)}, u32[]{:S(2)}, u32[]{:S(2)}) collective-permute-start(bf16[1024,256]{1,0:T(8,128)(2,1)S(1)} %bitcast.195), channel_id=1, source_target_pairs={{0,8},{8,0},{16,24},{24,16},{1,9},{9,1},{17,25},{25,17},{2,10},{10... | collective-permute-start | bytes 1572872 | tf_op jit(solution)/shard_map/ppermute | solution.py:42
  26.5 14.4 %collective-permute-start.4 = (bf16[1024,256]{1,0:T(8,128)(2,1)S(1)}, bf16[1024,256]{1,0:T(8,128)(2,1)S(1)}, u32[]{:S(2)}, u32[]{:S(2)}) collective-permute-start(bf16[1024,256]{1,0:T(8,128)(2,1)S(1)} %bitcast.196), channel_id=1, source_target_pairs={{0,1},{1,0},{2,3},{3,2},{4,5},{5,4},{6,7},{7,6},{8,9},{9,8},{10,11... | collective-permute-start | bytes 1572872 | tf_op jit(solution)/shard_map/ppermute | solution.py:86
  27.8 29.8 %all-to-all-start.1 = ((bf16[128,8,512]{0,2,1:T(8,128)(2,1)}), bf16[128,8,512]{0,2,1:T(8,128)(2,1)S(1)}, u32[]{:S(2)}, u32[]{:S(2)}) async-start(bf16[128,8,512]{0,2,1:T(8,128)(2,1)} %bitcast.16), calls=%async_computation.1 | async-start | bytes 2097152 | tf_op jit(solution)/shard_map/all_to_all | solution.py:203
  37.2 8.6 %collective-permute-start.10 = (bf16[512,256]{1,0:T(8,128)(2,1)S(1)}, bf16[512,256]{1,0:T(8,128)(2,1)S(1)}, u32[]{:S(2)}, u32[]{:S(2)}) collective-permute-start(bf16[512,256]{1,0:T(8,128)(2,1)S(1)} %slice.227), channel_id=1, source_target_pairs={{0,8},{8,0},{16,24},{24,16},{1,9},{9,1},{17,25},{25,17},{2,10},{10... | collective-permute-start | bytes 786440 | tf_op jit(solution)/shard_map/ppermute | solution.py:42
  38.7 7.0 %collective-permute-start.9 = (bf16[512,256]{1,0:T(8,128)(2,1)S(1)}, bf16[512,256]{1,0:T(8,128)(2,1)S(1)}, u32[]{:S(2)}, u32[]{:S(2)}) collective-permute-start(bf16[512,256]{1,0:T(8,128)(2,1)S(1)} %slice.226), channel_id=1, source_target_pairs={{0,16},{8,24},{16,0},{24,8},{1,17},{9,25},{17,1},{25,9},{2,18},{10... | collective-permute-start | bytes 786440 | tf_op jit(solution)/shard_map/ppermute | solution.py:42
  40.3 5.6 %collective-permute-start.8 = (bf16[1024,256]{1,0:T(8,128)(2,1)S(1)}, bf16[1024,256]{1,0:T(8,128)(2,1)S(1)}, u32[]{:S(2)}, u32[]{:S(2)}) collective-permute-start(bf16[1024,256]{1,0:T(8,128)(2,1)S(1)} %collective-permute-done.7), channel_id=1, source_target_pairs={{0,1},{1,0},{2,3},{3,2},{4,5},{5,4},{6,7},{7,6},{8,9},{9,8},{10,11... | collective-permute-start | bytes 1572872 | tf_op jit(solution)/shard_map/ppermute | solution.py:86
  40.3 5.5 %collective-permute-start.6 = (bf16[1024,256]{1,0:T(8,128)(2,1)S(1)}, bf16[1024,256]{1,0:T(8,128)(2,1)S(1)}, u32[]{:S(2)}, u32[]{:S(2)}) collective-permute-start(bf16[1024,256]{1,0:T(8,128)(2,1)S(1)} %collective-permute-done.5), channel_id=1, source_target_pairs={{0,1},{1,0},{2,3},{3,2},{4,5},{5,4},{6,7},{7,6},{8,9},{9,8},{10,11... | collective-permute-start | bytes 1572872 | tf_op jit(solution)/shard_map/ppermute | solution.py:86
  45.8 2.0 collective-permute-start.11
  58.3 5.6 %copy-start.8 = (f32[2048]{0:T(1024)S(1)}, f32[2048]{0:T(1024)}, u32[]{:S(2)}) copy-start(f32[2048]{0:T(1024)} %param.22) | copy-start | bytes 24580
  63.9 2.0 copy-start.2
  64.3 44.6 %copy-start.4 = (bf16[4,2,4,64,256]{4,3,2,0,1:T(8,128)(2,1)S(1)}, bf16[4,2,4,64,256]{4,3,2,0,1:T(8,128)(2,1)}, u32[]{:S(2)}) copy-start(bf16[4,2,4,64,256]{4,3,2,0,1:T(8,128)(2,1)} %fusion.32) | copy-start | bytes 3145732
  65.8 1.0 copy-start.5
  65.9 25.1 %collective-permute-start.13 = (bf16[256,2048]{1,0:T(8,128)(2,1)S(1)}, bf16[256,2048]{1,0:T(8,128)(2,1)S(1)}, u32[]{:S(2)}, u32[]{:S(2)}) collective-permute-start(bf16[256,2048]{1,0:T(8,128)(2,1)S(1)} %get-tuple-element.29), channel_id=1, source_target_pairs={{0,16},{8,24},{16,0},{24,8},{1,17},{9,25},{17,1},{25,9},{2,18},{10... | collective-permute-start | bytes 3145736 | tf_op jit(solution)/shard_map/ppermute | solution.py:42
  66.8 25.1 %collective-permute-start.12 = (bf16[256,2048]{1,0:T(8,128)(2,1)S(1)}, bf16[256,2048]{1,0:T(8,128)(2,1)S(1)}, u32[]{:S(2)}, u32[]{:S(2)}) collective-permute-start(bf16[256,2048]{1,0:T(8,128)(2,1)S(1)} %get-tuple-element.29), channel_id=1, source_target_pairs={{0,8},{8,0},{16,24},{24,16},{1,9},{9,1},{17,25},{25,17},{2,10},{10... | collective-permute-start | bytes 3145736 | tf_op jit(solution)/shard_map/ppermute | solution.py:42
  91.0 2.4 %copy-start.6 = (bf16[256,2048]{1,0:T(8,128)(2,1)}, bf16[256,2048]{1,0:T(8,128)(2,1)S(1)}, u32[]{:S(2)}) copy-start(bf16[256,2048]{1,0:T(8,128)(2,1)S(1)} %collective-permute-done.13) | copy-start | bytes 3145732
  91.9 1.5 copy-start.7
  92.0 15.0 %collective-permute-start.15 = (bf16[128,2048]{1,0:T(8,128)(2,1)S(1)}, bf16[128,2048]{1,0:T(8,128)(2,1)}, u32[]{:S(2)}, u32[]{:S(2)}) collective-permute-start(bf16[128,2048]{1,0:T(8,128)(2,1)S(1)} %slice.189), channel_id=1, source_target_pairs={{0,8},{8,0},{16,24},{24,16},{1,9},{9,1},{17,25},{25,17},{2,10},{10... | collective-permute-start | bytes 1572872 | tf_op jit(solution)/shard_map/ppermute | solution.py:42
  92.6 14.9 %collective-permute-start.14 = (bf16[128,2048]{1,0:T(8,128)(2,1)S(1)}, bf16[128,2048]{1,0:T(8,128)(2,1)}, u32[]{:S(2)}, u32[]{:S(2)}) collective-permute-start(bf16[128,2048]{1,0:T(8,128)(2,1)S(1)} %slice.188), channel_id=1, source_target_pairs={{0,16},{8,24},{16,0},{24,8},{1,17},{9,25},{17,1},{25,9},{2,18},{10... | collective-permute-start | bytes 1572872 | tf_op jit(solution)/shard_map/ppermute | solution.py:42
  93.6 34.3 %collective-permute-start.17 = (bf16[256,2048]{1,0:T(8,128)(2,1)S(1)}, bf16[256,2048]{1,0:T(8,128)(2,1)S(1)}, u32[]{:S(2)}, u32[]{:S(2)}) collective-permute-start(bf16[256,2048]{1,0:T(8,128)(2,1)S(1)} %get-tuple-element.35), channel_id=1, source_target_pairs={{0,16},{8,24},{16,0},{24,8},{1,17},{9,25},{17,1},{25,9},{2,18},{10... | collective-permute-start | bytes 3145736 | tf_op jit(solution)/shard_map/ppermute | solution.py:42
  94.8 33.0 %collective-permute-start.16 = (bf16[256,2048]{1,0:T(8,128)(2,1)S(1)}, bf16[256,2048]{1,0:T(8,128)(2,1)S(1)}, u32[]{:S(2)}, u32[]{:S(2)}) collective-permute-start(bf16[256,2048]{1,0:T(8,128)(2,1)S(1)} %get-tuple-element.35), channel_id=1, source_target_pairs={{0,8},{8,0},{16,24},{24,16},{1,9},{9,1},{17,25},{25,17},{2,10},{10... | collective-permute-start | bytes 3145736 | tf_op jit(solution)/shard_map/ppermute | solution.py:42
  107.5 5.0 %slice-start = ((s8[8388608]{0:T(1024)(128)(4,1)}), s8[4194304]{0:T(1024)(128)(4,1)S(1)}, s32[]{:S(2)}) async-start(s8[8388608]{0:T(1024)(128)(4,1)} %bitcast.208), calls=%async_computation.2 | async-start | bytes 8388608
  109.0 3.6 %slice-start.1 = ((s8[8388608]{0:T(1024)(128)(4,1)}), s8[4194304]{0:T(1024)(128)(4,1)S(1)}, s32[]{:S(2)}) async-start(s8[8388608]{0:T(1024)(128)(4,1)} %bitcast.208), calls=%async_computation.3 | async-start | bytes 8388608
  127.9 14.4 %collective-permute-start.19 = (bf16[128,2048]{1,0:T(8,128)(2,1)S(1)}, bf16[128,2048]{1,0:T(8,128)(2,1)S(1)}, u32[]{:S(2)}, u32[]{:S(2)}) collective-permute-start(bf16[128,2048]{1,0:T(8,128)(2,1)S(1)} %slice.193), channel_id=1, source_target_pairs={{0,8},{8,0},{16,24},{24,16},{1,9},{9,1},{17,25},{25,17},{2,10},{10... | collective-permute-start | bytes 1572872 | tf_op jit(solution)/shard_map/ppermute | solution.py:42
  129.5 14.8 %collective-permute-start.18 = (bf16[128,2048]{1,0:T(8,128)(2,1)S(1)}, bf16[128,2048]{1,0:T(8,128)(2,1)S(1)}, u32[]{:S(2)}, u32[]{:S(2)}) collective-permute-start(bf16[128,2048]{1,0:T(8,128)(2,1)S(1)} %slice.192), channel_id=1, source_target_pairs={{0,16},{8,24},{16,0},{24,8},{1,17},{9,25},{17,1},{25,9},{2,18},{10... | collective-permute-start | bytes 1572872 | tf_op jit(solution)/shard_map/ppermute | solution.py:42
  137.5 22.9 %collective-permute-start.23 = (bf16[128,2048]{1,0:T(8,128)(2,1)S(1)}, bf16[128,2048]{1,0:T(8,128)(2,1)S(1)}, u32[]{:S(2)}, u32[]{:S(2)}) collective-permute-start(bf16[128,2048]{1,0:T(8,128)(2,1)S(1)} %get-tuple-element.55), channel_id=1, source_target_pairs={{0,8},{8,0},{16,24},{24,16},{1,9},{9,1},{17,25},{25,17},{2,10},{10... | collective-permute-start | bytes 1572872 | tf_op jit(solution)/shard_map/ppermute | solution.py:42
  138.1 22.3 %collective-permute-start.22 = (bf16[128,2048]{1,0:T(8,128)(2,1)S(1)}, bf16[128,2048]{1,0:T(8,128)(2,1)S(1)}, u32[]{:S(2)}, u32[]{:S(2)}) collective-permute-start(bf16[128,2048]{1,0:T(8,128)(2,1)S(1)} %get-tuple-element.56), channel_id=1, source_target_pairs={{0,16},{8,24},{16,0},{24,8},{1,17},{9,25},{17,1},{25,9},{2,18},{10... | collective-permute-start | bytes 1572872 | tf_op jit(solution)/shard_map/ppermute | solution.py:42
  139.6 23.9 %collective-permute-start.21 = (bf16[128,2048]{1,0:T(8,128)(2,1)S(1)}, bf16[128,2048]{1,0:T(8,128)(2,1)S(1)}, u32[]{:S(2)}, u32[]{:S(2)}) collective-permute-start(bf16[128,2048]{1,0:T(8,128)(2,1)S(1)} %get-tuple-element.57), channel_id=1, source_target_pairs={{0,16},{8,24},{16,0},{24,8},{1,17},{9,25},{17,1},{25,9},{2,18},{10... | collective-permute-start | bytes 1572872 | tf_op jit(solution)/shard_map/ppermute | solution.py:42
  142.4 21.2 %collective-permute-start.20 = (bf16[128,2048]{1,0:T(8,128)(2,1)S(1)}, bf16[128,2048]{1,0:T(8,128)(2,1)S(1)}, u32[]{:S(2)}, u32[]{:S(2)}) collective-permute-start(bf16[128,2048]{1,0:T(8,128)(2,1)S(1)} %get-tuple-element.58), channel_id=1, source_target_pairs={{0,8},{8,0},{16,24},{24,16},{1,9},{9,1},{17,25},{25,17},{2,10},{10... | collective-permute-start | bytes 1572872 | tf_op jit(solution)/shard_map/ppermute | solution.py:42
  145.9 6.2 %slice-start.2 = ((s8[8388608]{0:T(1024)(128)(4,1)}), s8[4194304]{0:T(1024)(128)(4,1)S(1)}, s32[]{:S(2)}) async-start(s8[8388608]{0:T(1024)(128)(4,1)} %bitcast.210), calls=%async_computation.4 | async-start | bytes 8388608
  146.2 5.9 %slice-start.3 = ((s8[8388608]{0:T(1024)(128)(4,1)}), s8[4194304]{0:T(1024)(128)(4,1)S(1)}, s32[]{:S(2)}) async-start(s8[8388608]{0:T(1024)(128)(4,1)} %bitcast.210), calls=%async_computation.5 | async-start | bytes 8388608
  164.9 45.8 %copy-start.3 = (f32[512,2048]{1,0:T(8,128)S(1)}, f32[512,2048]{1,0:T(8,128)}, u32[]{:S(2)}) copy-start(f32[512,2048]{1,0:T(8,128)} %copy-done.2) | copy-start | bytes 12582916
  165.1 14.9 %collective-permute-start.29 = (bf16[128,2048]{1,0:T(8,128)(2,1)S(1)}, bf16[128,2048]{1,0:T(8,128)(2,1)S(1)}, u32[]{:S(2)}, u32[]{:S(2)}) collective-permute-start(bf16[128,2048]{1,0:T(8,128)(2,1)S(1)} %get-tuple-element.49), channel_id=1, source_target_pairs={{0,8},{8,0},{16,24},{24,16},{1,9},{9,1},{17,25},{25,17},{2,10},{10... | collective-permute-start | bytes 1572872 | tf_op jit(solution)/shard_map/ppermute | solution.py:42
  165.8 14.8 %collective-permute-start.27 = (bf16[128,2048]{1,0:T(8,128)(2,1)S(1)}, bf16[128,2048]{1,0:T(8,128)(2,1)S(1)}, u32[]{:S(2)}, u32[]{:S(2)}) collective-permute-start(bf16[128,2048]{1,0:T(8,128)(2,1)S(1)} %get-tuple-element.51), channel_id=1, source_target_pairs={{0,16},{8,24},{16,0},{24,8},{1,17},{9,25},{17,1},{25,9},{2,18},{10... | collective-permute-start | bytes 1572872 | tf_op jit(solution)/shard_map/ppermute | solution.py:42
  166.0 25.2 %collective-permute-start.24 = (bf16[128,2048]{1,0:T(8,128)(2,1)S(1)}, bf16[128,2048]{1,0:T(8,128)(2,1)S(1)}, u32[]{:S(2)}, u32[]{:S(2)}) collective-permute-start(bf16[128,2048]{1,0:T(8,128)(2,1)S(1)} %get-tuple-element.39), channel_id=1, source_target_pairs={{0,8},{8,0},{16,24},{24,16},{1,9},{9,1},{17,25},{25,17},{2,10},{10... | collective-permute-start | bytes 1572872 | tf_op jit(solution)/shard_map/ppermute | solution.py:42
  167.5 24.3 %collective-permute-start.25 = (bf16[128,2048]{1,0:T(8,128)(2,1)S(1)}, bf16[128,2048]{1,0:T(8,128)(2,1)S(1)}, u32[]{:S(2)}, u32[]{:S(2)}) collective-permute-start(bf16[128,2048]{1,0:T(8,128)(2,1)S(1)} %get-tuple-element.40), channel_id=1, source_target_pairs={{0,16},{8,24},{16,0},{24,8},{1,17},{9,25},{17,1},{25,9},{2,18},{10... | collective-permute-start | bytes 1572872 | tf_op jit(solution)/shard_map/ppermute | solution.py:42
  169.3 33.8 %collective-permute-start.31 = (bf16[128,2048]{1,0:T(8,128)(2,1)S(1)}, bf16[128,2048]{1,0:T(8,128)(2,1)S(1)}, u32[]{:S(2)}, u32[]{:S(2)}) collective-permute-start(bf16[128,2048]{1,0:T(8,128)(2,1)S(1)} %get-tuple-element.50), channel_id=1, source_target_pairs={{0,16},{8,24},{16,0},{24,8},{1,17},{9,25},{17,1},{25,9},{2,18},{10... | collective-permute-start | bytes 1572872 | tf_op jit(solution)/shard_map/ppermute | solution.py:42
  180.0 23.0 %collective-permute-start.26 = (bf16[128,2048]{1,0:T(8,128)(2,1)S(1)}, bf16[128,2048]{1,0:T(8,128)(2,1)S(1)}, u32[]{:S(2)}, u32[]{:S(2)}) collective-permute-start(bf16[128,2048]{1,0:T(8,128)(2,1)S(1)} %get-tuple-element.52), channel_id=1, source_target_pairs={{0,8},{8,0},{16,24},{24,16},{1,9},{9,1},{17,25},{25,17},{2,10},{10... | collective-permute-start | bytes 1572872 | tf_op jit(solution)/shard_map/ppermute | solution.py:42
  180.9 29.7 %collective-permute-start.30 = (bf16[128,2048]{1,0:T(8,128)(2,1)S(1)}, bf16[128,2048]{1,0:T(8,128)(2,1)S(1)}, u32[]{:S(2)}, u32[]{:S(2)}) collective-permute-start(bf16[128,2048]{1,0:T(8,128)(2,1)S(1)} %get-tuple-element.47), channel_id=1, source_target_pairs={{0,16},{8,24},{16,0},{24,8},{1,17},{9,25},{17,1},{25,9},{2,18},{10... | collective-permute-start | bytes 1572872 | tf_op jit(solution)/shard_map/ppermute | solution.py:42
  191.2 19.4 %collective-permute-start.28 = (bf16[128,2048]{1,0:T(8,128)(2,1)S(1)}, bf16[128,2048]{1,0:T(8,128)(2,1)S(1)}, u32[]{:S(2)}, u32[]{:S(2)}) collective-permute-start(bf16[128,2048]{1,0:T(8,128)(2,1)S(1)} %get-tuple-element.48), channel_id=1, source_target_pairs={{0,8},{8,0},{16,24},{24,16},{1,9},{9,1},{17,25},{25,17},{2,10},{10... | collective-permute-start | bytes 1572872 | tf_op jit(solution)/shard_map/ppermute | solution.py:42
  210.7 3.4 %copy-start.1 = (bf16[128,2048]{1,0:T(8,128)(2,1)S(1)}, bf16[128,2048]{1,0:T(8,128)(2,1)}, u32[]{:S(2)}) copy-start(bf16[128,2048]{1,0:T(8,128)(2,1)} %param.20) | copy-start | bytes 1572868
where the time goes:
time: 218 us; the launch traced here: 214 us
  waiting for transfers between devices  99.8 us (46%)
  starting transfers between devices  43.2 us (20%)
  matrix products  41.2 us (19%)
  other arithmetic  15 us (7%)
  local copies, waits for them, and re-layouts  14.1 us (6%)
    ppermute x27, waiting for transfers between devices, neighbour(): lax.ppermute(value, 'sp', [(source, source ^ bit) for source in range(cou...  92.4 us
    ppermute x27, starting transfers between devices, neighbour(): lax.ppermute(value, 'sp', [(source, source ^ bit) for source in range(cou...  27.2 us
    dot_general x2, matrix products, experts_on(): jnp.einsum('emf,efd->emd', hidden, w_down, preferred_element_type=jnp.flo...  11.5 us
    unnamed x46, local copies, waits for them, and re-layouts  8.38 us
    dot_general x2, matrix products, experts_on(): jnp.einsum('emd,edf->emf', packed, w_up, preferred_element_type=jnp.float32)  8.31 us
    dot_general x2, matrix products, experts_on(): jnp.einsum('emd,edf->emf', packed, w_gate, preferred_element_type=jnp.flo...  8.19 us
    all_to_all x1, starting transfers between devices, body(): lax.all_to_all(head_normed, 'tp', split_axis=1, concat_axis=0, tiled=True)  6.69 us
    dot_general x1, matrix products, mix(): lax.dot_general(by_row, jnp.concatenate(order, axis=1), (((0,), (0,)), ((...  5.55 us
  transfers between devices with their start and end apart: 34, of which 17 were waited for; matrix products, arithmetic and copies ran while one was open for 26% of the time, Pallas kernels for 0%

commit v1 on v0

--- a/solution.py
+++ b/solution.py
@@ -1,6 +1,10 @@
+import functools
+
 import jax
 import jax.numpy as jnp
 from jax import lax
+from jax.experimental import pallas as pl
+from jax.experimental.pallas import tpu as pltpu
 from jax.sharding import PartitionSpec as P
 
 HEAD = 64
@@ -71,48 +75,11 @@
     return (left.astype(jnp.float32) + right.astype(jnp.float32)).astype(jnp.bfloat16)
 
 
-def every_column(out_proj):
-    me, tp_count = lax.axis_index("sp"), lax.axis_size("tp")
-    rows, width = out_proj.shape
-    mine = lax.dynamic_slice_in_dim(out_proj, me * (width // 4), width // 4, axis=1)
-    mine = jnp.transpose(mine.reshape(rows, 2, width // 8), (1, 0, 2))
-    mine = jnp.tile(mine, (tp_count // 2, 1, 1))
-    mine = lax.all_to_all(mine, "tp", split_axis=0, concat_axis=0, tiled=True)
-    return mine.reshape(tp_count * rows, width // 8)
-
-
-def other_core(value):
-    count = lax.axis_size("tp")
-    return lax.ppermute(value, "tp", [(source, source ^ 1) for source in range(count)])
-
-
-def mix(by_row, mine):
-    parts = []
-    for part in gather_far(*gather_near(mine)):
-        parts.extend([part, other_core(part)])
-    stacked = jnp.stack(parts)
-    me, core = lax.axis_index("sp"), lax.axis_index("tp") % 2
-    order = [
-        stacked[2 * (me ^ column) + (core ^ parity)] for column in range(4) for parity in range(2)
-    ]
-    return lax.dot_general(
-        by_row,
-        jnp.concatenate(order, axis=1),
-        (((0,), (0,)), ((), ())),
-        preferred_element_type=jnp.float32,
-    )
-
-
-def route_lists(route_ids, route_weight):
-    listing = jnp.concatenate([route_ids.astype(jnp.float32), route_weight], axis=1).T
-    return jnp.stack([listing] + [neighbour(listing, distance) for distance in range(1, 4)])
-
-
-def route_tables(everyone, local_experts, half, slot):
+def route_tables(ids, weights, local_experts, half, slot):
     me = lax.axis_index("sp")
-    top = everyone.shape[1] // 2
-    ids = everyone[:, :top].astype(jnp.int32).reshape(4, top, -1, half)
-    weights = everyone[:, top:].reshape(4, top, -1, half)
+    top = ids.shape[1]
+    ids = ids.reshape(4, top, -1, half)
+    weights = weights.reshape(4, top, -1, half)
     experts = me * local_experts + jnp.arange(local_experts, dtype=jnp.int32)
     hit = ids[:, :, :, None, :] == experts[None, None, None, :, None]
     marks = jnp.any(hit, axis=1)
@@ -150,6 +117,470 @@
     return total.astype(jnp.bfloat16), held
 
 
+MESH = pl.DeviceIdType.MESH
+SUB = 128
+
+
+def front_kernel(
+    tp_count,
+    conv_in,
+    in_gate,
+    out_gate,
+    doc_ids,
+    taps_in,
+    gain_in,
+    out_proj,
+    resid,
+    norm_gain_in,
+    ids,
+    weights,
+    rows_out,
+    later_out,
+    stream_out,
+    ids_out,
+    weights_out,
+    in_buf,
+    gate_buf,
+    after_buf,
+    doc_buf,
+    taps,
+    gain,
+    norm_gain,
+    proj,
+    resid_buf,
+    spread,
+    outgoing,
+    by_row,
+    gathered,
+    later,
+    stream,
+    local_sem,
+    out_sem,
+    edge_send,
+    edge_recv,
+    list_send,
+    list_recv,
+    slice_send,
+    slice_recv,
+    plane_send,
+    plane_recv,
+    corner_send,
+    corner_recv,
+    core_send,
+    core_recv,
+    trade_send,
+    trade_recv,
+    near_send,
+    near_recv,
+    far_send,
+    far_recv,
+):
+    sp, tp = lax.axis_index("sp"), lax.axis_index("tp")
+    z, core = tp // 2, tp % 2
+    channels, width = out_proj.shape
+    rows = resid.shape[0]
+    half, subs = rows // 2, rows // SUB
+    first = half // SUB
+    planes = tp_count // 2
+    near_of = [sp ^ 1, sp ^ 2]
+    diagonal = sp ^ 3
+    pending = []
+
+    def remote(source, target, send_sem, recv_sem, to_sp, to_tp):
+        return pltpu.make_async_remote_copy(
+            src_ref=source,
+            dst_ref=target,
+            send_sem=send_sem,
+            recv_sem=recv_sem,
+            device_id=(to_sp, to_tp),
+            device_id_type=MESH,
+        )
+
+    def send(source, target, send_sem, recv_sem, to_sp, to_tp):
+        copy = remote(source, target, send_sem, recv_sem, to_sp, to_tp)
+        copy.start()
+        pending.append(copy)
+
+    def arrive(region, send_sem, recv_sem):
+        remote(region, region, send_sem, recv_sem, near_of[0], tp).wait_recv()
+
+    tail = conv_in.shape[1] - SUB
+    loads = [
+        pltpu.make_async_copy(conv_in, in_buf.at[:, pl.ds(SUB, conv_in.shape[1])], local_sem.at[0]),
+        pltpu.make_async_copy(in_gate, gate_buf.at[:, pl.ds(SUB, conv_in.shape[1])], local_sem.at[1]),
+        pltpu.make_async_copy(out_gate, after_buf, local_sem.at[2]),
+        pltpu.make_async_copy(doc_ids, doc_buf.at[:, pl.ds(SUB, conv_in.shape[1])], local_sem.at[3]),
+        pltpu.make_async_copy(taps_in, taps, local_sem.at[6]),
+        pltpu.make_async_copy(gain_in, gain, local_sem.at[7]),
+        pltpu.make_async_copy(
+            out_proj, proj.at[pl.ds(pl.multiple_of(tp * channels, channels), channels)], local_sem.at[4]
+        ),
+        pltpu.make_async_copy(resid, resid_buf, local_sem.at[5]),
+        pltpu.make_async_copy(norm_gain_in, norm_gain, local_sem.at[8]),
+        pltpu.make_async_copy(ids, ids_out.at[0], local_sem.at[9]),
+        pltpu.make_async_copy(weights, weights_out.at[0], local_sem.at[10]),
+    ]
+    for copy in loads:
+        copy.start()
+
+    barrier = pltpu.get_barrier_semaphore()
+    for d in range(1, tp_count):
+        pl.semaphore_signal(barrier, inc=1, device_id=(sp, tp ^ d), device_id_type=MESH)
+    for d in range(1, 4):
+        pl.semaphore_signal(barrier, inc=1, device_id=(sp ^ d, tp), device_id_type=MESH)
+    pl.semaphore_wait(barrier, tp_count + 2)
+
+    after, before = (sp + 1) % 4, (sp + 3) % 4
+    edge = pl.ds(0, SUB)
+    for at, (source, target) in enumerate(
+        ((conv_in, in_buf), (in_gate, gate_buf), (doc_ids, doc_buf))
+    ):
+        send(
+            source.at[:, pl.ds(tail, SUB)],
+            target.at[:, edge],
+            edge_send.at[at],
+            edge_recv.at[at],
+            after,
+            tp,
+        )
+
+    eighth = width // 8
+
+    def columns(place, side):
+        return pl.ds(pl.multiple_of(place * (2 * eighth) + side * eighth, eighth), eighth)
+
+    my_rows = pl.ds(pl.multiple_of(tp * channels, channels), channels)
+    slices = []
+    for d in range(2, tp_count):
+        side = core ^ (d & 1)
+        copy = remote(
+            out_proj.at[:, columns(sp, side)],
+            proj.at[my_rows, columns(sp, side)],
+            slice_send.at[d],
+            slice_recv.at[d],
+            sp,
+            tp ^ d,
+        )
+        copy.start()
+        slices.append(copy)
+    send(out_proj, proj.at[my_rows], slice_send.at[1], slice_recv.at[1], sp, tp ^ 1)
+    for d in range(1, 4):
+        send(ids, ids_out.at[d], list_send.at[0, d], list_recv.at[0, d], sp ^ d, tp)
+        send(weights, weights_out.at[d], list_send.at[1, d], list_recv.at[1, d], sp ^ d, tp)
+    for copy in loads[:6]:
+        copy.wait()
+    for k in range(3):
+        spread[k] = jnp.broadcast_to(taps[k : k + 1, :], (channels, channels)).T
+    spread[3] = jnp.broadcast_to(gain[...], (channels, channels)).T
+    def piece(owner, q):
+        base = pl.multiple_of(owner * rows + q * SUB, SUB)
+        wide = pl.ds(base, 2 * SUB)
+        gated = gate_buf[:, wide].astype(jnp.float32) * in_buf[:, wide].astype(jnp.float32)
+        docs = jnp.broadcast_to(doc_buf[:, wide], (8, 2 * SUB))
+        now = docs[:, SUB:]
+        same_one = (pltpu.roll(docs, 1, 1)[:, SUB:] == now).astype(jnp.float32)[:1]
+        same_two = (pltpu.roll(docs, 2, 1)[:, SUB:] == now).astype(jnp.float32)[:1]
+        conv = (
+            spread[2] * gated[:, SUB:]
+            + spread[1] * (pltpu.roll(gated, 1, 1)[:, SUB:] * same_one)
+            + spread[0] * (pltpu.roll(gated, 2, 1)[:, SUB:] * same_two)
+        )
+        gated_out = after_buf[:, pl.ds(base, SUB)].astype(jnp.float32) * conv
+        by_head = gated_out.reshape(channels // HEAD, HEAD, SUB)
+        by_head = by_head * lax.rsqrt(
+            jnp.mean(by_head * by_head, axis=1, keepdims=True) + norm_eps
+        )
+        normed = by_head.reshape(channels, SUB) * spread[3]
+        return normed.T.astype(jnp.bfloat16)
+
+    my_channels = pl.ds(pl.multiple_of(tp * channels, channels), channels)
+
+    def trade(q, d):
+        return remote(
+            outgoing.at[q, d],
+            by_row.at[q, :, my_channels],
+            trade_send.at[q, d],
+            trade_recv.at[q, d],
+            sp,
+            tp ^ d,
+        )
+
+    def start_trade(q):
+        def begin(at, carry):
+            trade(q, tp_count - 1 - at).start()
+            return carry
+
+        lax.fori_loop(0, tp_count - 1, begin, 0)
+
+    def sent_trade(q):
+        def sent(d, carry):
+            trade(q, d).wait_send()
+            return carry
+
+        lax.fori_loop(1, tp_count, sent, 0)
+
+    def block_rows(step):
+        deep = 2 * channels
+        return pl.ds(pl.multiple_of((z ^ step) * deep, deep), deep)
+
+    def part_rows(step, upper):
+        deep = 2 * channels
+        return pl.ds(pl.multiple_of((z ^ step) * deep + upper * channels, channels), channels)
+
+    def spread_slice(step):
+        arrive_rows = [
+            pl.ds(pl.multiple_of((tp ^ (2 * step + odd)) * channels, channels), channels)
+            for odd in range(2)
+        ]
+        for odd in range(2):
+            d = 2 * step + odd
+            arrive(
+                proj.at[arrive_rows[odd], columns(sp, core)], slice_send.at[d], slice_recv.at[d]
+            )
+        region = proj.at[block_rows(step), columns(sp, core)]
+        for k in range(2):
+            send(region, region, plane_send.at[k, step], plane_recv.at[k, step], near_of[k], tp)
+        send(region, region, core_send.at[0, step], core_recv.at[0, step], sp, tp ^ 1)
+
+    def spread_plane(step):
+        for k in range(2):
+            region = proj.at[block_rows(step), columns(near_of[k], core)]
+            arrive(region, plane_send.at[k, step], plane_recv.at[k, step])
+            part = proj.at[part_rows(step, k), columns(near_of[k], core)]
+            send(part, part, corner_send.at[k, step], corner_recv.at[k, step], near_of[1 - k], tp)
+            send(region, region, core_send.at[1 + k, step], core_recv.at[1 + k, step], sp, tp ^ 1)
+
+    def spread_corner(step):
+        for k in range(2):
+            arrive(
+                proj.at[part_rows(step, k), columns(diagonal, core)],
+                corner_send.at[k, step],
+                corner_recv.at[k, step],
+            )
+        region = proj.at[block_rows(step), columns(diagonal, core)]
+        send(region, region, core_send.at[3, step], core_recv.at[3, step], sp, tp ^ 1)
+
+    def others_done(step):
+        other = 1 - core
+        for k, place in enumerate((sp, near_of[0], near_of[1], diagonal)):
+            arrive(
+                proj.at[block_rows(step), columns(place, other)],
+                core_send.at[k, step],
+                core_recv.at[k, step],
+            )
+
+    order = [1, 0, *range(2, subs)]
+
+    def convolve(q):
+        def one(at, carry):
+            d = tp_count - 1 - at
+            outgoing[q, d] = piece(tp ^ d, q)
+            return carry
+
+        lax.fori_loop(0, tp_count - 1, one, 0)
+        by_row[q, :, my_channels] = piece(tp, q)
+
+    for q in range(1, subs):
+        convolve(q)
+    for step in range(1, planes):
+        if step == planes - 1:
+            for copy in slices:
+                copy.wait_send()
+            start_trade(order[0])
+        spread_slice(step)
+    for step in range(1, planes):
+        spread_plane(step)
+    for at, target in enumerate((in_buf, gate_buf, doc_buf)):
+        arrive(target.at[:, edge], edge_send.at[at], edge_recv.at[at])
+    doc_buf[:, edge] = jnp.where(sp == 0, -1, doc_buf[:, edge])
+    convolve(0)
+    for step in range(1, planes):
+        spread_corner(step)
+    sent_trade(order[0])
+    start_trade(order[1])
+    for copy in loads[6:]:
+        copy.wait()
+    arrive(
+        proj.at[pl.ds(pl.multiple_of((tp ^ 1) * channels, channels), channels)],
+        slice_send.at[1],
+        slice_recv.at[1],
+    )
+    for step in range(1, planes):
+        others_done(step)
+
+    tile = width // 4
+    stores = []
+    for at_q, q in enumerate(order):
+        if at_q > 0:
+            sent_trade(q)
+            if at_q + 1 < subs:
+                start_trade(order[at_q + 1])
+
+        def got(d, carry, q=q):
+            theirs = pl.ds(pl.multiple_of((tp ^ d) * channels, channels), channels)
+            arrive(by_row.at[q, :, theirs], trade_send.at[q, d], trade_recv.at[q, d])
+            return carry
+
+        lax.fori_loop(1, tp_count, got, 0)
+        mine = pl.ds(q * SUB, SUB)
+
+        def project(n, total, q=q, mine=mine):
+            cols = pl.ds(pl.multiple_of(n * tile, tile), tile)
+            value = resid_buf[mine, cols].astype(jnp.float32) + jnp.dot(
+                by_row[q], proj[:, cols], preferred_element_type=jnp.float32
+            )
+            stream[mine, cols] = value
+            return total + jnp.sum(value * value, axis=1, keepdims=True)
+
+        total = lax.fori_loop(0, 4, project, jnp.zeros((SUB, 1), jnp.float32))
+        scale = lax.rsqrt(total / width + norm_eps)
+
+        def normalize(n, carry, q=q, mine=mine, scale=scale):
+            cols = pl.ds(pl.multiple_of(n * tile, tile), tile)
+            value = (stream[mine, cols] * scale * norm_gain[:, cols]).astype(jnp.bfloat16)
+            if q < first:
+                gathered[0, mine, cols] = value
+            else:
+                later[pl.ds((q - first) * SUB, SUB), cols] = value
+            return carry
+
+        lax.fori_loop(0, 4, normalize, 0)
+        if q < first:
+            region = gathered.at[0, mine]
+            for k in range(2):
+                send(
+                    region,
+                    gathered.at[1 + k, mine],
+                    near_send.at[k, q],
+                    near_recv.at[k, q],
+                    near_of[k],
+                    tp,
+                )
+    stores.append(pltpu.make_async_copy(stream, stream_out, out_sem.at[0]))
+    stores.append(pltpu.make_async_copy(later, later_out, out_sem.at[1]))
+    stores.append(pltpu.make_async_copy(gathered.at[0], rows_out.at[0], out_sem.at[2]))
+    for copy in stores:
+        copy.start()
+    for d in range(1, 4):
+        arrive(ids_out.at[d], list_send.at[0, d], list_recv.at[0, d])
+        arrive(weights_out.at[d], list_send.at[1, d], list_recv.at[1, d])
+
+    for q in range(first):
+        for k in range(2):
+            arrive(
+                gathered.at[1 + k, pl.ds(q * SUB, SUB)], near_send.at[k, q], near_recv.at[k, q]
+            )
+            part = pl.ds(q * SUB + k * (SUB // 2), SUB // 2)
+            send(
+                gathered.at[1 + k, part],
+                gathered.at[3, part],
+                far_send.at[k, q],
+                far_recv.at[k, q],
+                near_of[1 - k],
+                tp,
+            )
+    for k in range(2):
+        store = pltpu.make_async_copy(gathered.at[1 + k], rows_out.at[1 + k], out_sem.at[3 + k])
+        store.start()
+        stores.append(store)
+    for q in range(first):
+        for k in range(2):
+            part = pl.ds(q * SUB + k * (SUB // 2), SUB // 2)
+            arrive(gathered.at[3, part], far_send.at[k, q], far_recv.at[k, q])
+        store = pltpu.make_async_copy(
+            gathered.at[3, pl.ds(q * SUB, SUB)],
+            rows_out.at[3, pl.ds(q * SUB, SUB)],
+            out_sem.at[5 + q],
+        )
+        store.start()
+        stores.append(store)
+    for copy in stores:
+        copy.wait()
+    for copy in pending:
+        copy.wait_send()
+
+
+def front(
+    conv_in, in_gate, out_gate, doc_ids, conv_taps, head_gain, out_proj, resid, norm_gain,
+    route_ids, route_weight,
+):
+    tp_count = lax.axis_size("tp")
+    channels, width = out_proj.shape
+    positions = conv_in.shape[1]
+    rows = resid.shape[0]
+    half, subs = rows // 2, rows // SUB
+    first, planes = half // SUB, tp_count // 2
+    top = route_ids.shape[1]
+    hbm = pl.BlockSpec(memory_space=pltpu.HBM)
+    vmem = pl.BlockSpec(memory_space=pltpu.VMEM)
+    dma = pltpu.SemaphoreType.DMA
+    return pl.pallas_call(
+        functools.partial(front_kernel, tp_count),
+        out_shape=(
+            jax.ShapeDtypeStruct((4, half, width), jnp.bfloat16),
+            jax.ShapeDtypeStruct((half, width), jnp.bfloat16),
+            jax.ShapeDtypeStruct((rows, width), jnp.float32),
+            jax.ShapeDtypeStruct((4, top, rows), jnp.int32),
+            jax.ShapeDtypeStruct((4, top, rows), jnp.float32),
+        ),
+        in_specs=[hbm] * 11,
+        out_specs=(hbm, hbm, hbm, vmem, vmem),
+        scratch_shapes=[
+            pltpu.VMEM((channels, SUB + positions), jnp.bfloat16),
+            pltpu.VMEM((channels, SUB + positions), jnp.bfloat16),
+            pltpu.VMEM((channels, positions), jnp.bfloat16),
+            pltpu.VMEM((1, SUB + positions), jnp.int32),
+            pltpu.VMEM((3, channels), jnp.float32),
+            pltpu.VMEM((1, channels), jnp.float32),
+            pltpu.VMEM((1, width), jnp.float32),
+            pltpu.VMEM((tp_count * channels, width), jnp.bfloat16),
+            pltpu.VMEM((rows, width), jnp.bfloat16),
+            pltpu.VMEM((4, channels, SUB), jnp.float32),
+            pltpu.VMEM((subs, tp_count, SUB, channels), jnp.bfloat16),
+            pltpu.VMEM((subs, SUB, tp_count * channels), jnp.bfloat16),
+            pltpu.VMEM((4, half, width), jnp.bfloat16),
+            pltpu.VMEM((half, width), jnp.bfloat16),
+            pltpu.VMEM((rows, width), jnp.float32),
+            dma((11,)),
+            dma((5 + first,)),
+            dma((3,)),
+            dma((3,)),
+            dma((2, 4)),
+            dma((2, 4)),
+            dma((tp_count,)),
+            dma((tp_count,)),
+            dma((2, planes)),
+            dma((2, planes)),
+            dma((2, planes)),
+            dma((2, planes)),
+            dma((4, planes)),
+            dma((4, planes)),
+            dma((subs, tp_count)),
+            dma((subs, tp_count)),
+            dma((2, first)),
+            dma((2, first)),
+            dma((2, first)),
+            dma((2, first)),
+        ],
+        compiler_params=pltpu.CompilerParams(
+            collective_id=0, has_side_effects=True, vmem_limit_bytes=60 * 1024 * 1024
+        ),
+        name="front",
+    )(
+        conv_in,
+        in_gate,
+        out_gate,
+        doc_ids[None],
+        conv_taps.T,
+        head_gain[None],
+        out_proj,
+        resid,
+        norm_gain[None],
+        route_ids.T,
+        route_weight.T,
+    )
+
+
 def body(
     conv_in,
     in_gate,
@@ -166,62 +597,38 @@
     w_up,
     w_down,
 ):
-    gated_in = in_gate.astype(jnp.float32) * conv_in.astype(jnp.float32)
-    doc_value = doc_ids.astype(jnp.float32)
-    edge = jnp.concatenate([gated_in[:, -2:], doc_value[None, -2:]], axis=0)
-    edge = shifted(edge, "sp", 1)
-    earlier_in, earlier_doc = edge[:-1], edge[-1]
-    padded_in = jnp.concatenate([earlier_in, gated_in], axis=1)
-    padded_doc = jnp.concatenate([earlier_doc, doc_value])
-    same_one = (padded_doc[1:-1] == doc_value).astype(jnp.float32)
-    same_two = (padded_doc[:-2] == doc_value).astype(jnp.float32)
-    conv_out = (
-        conv_taps[:, 2:3] * gated_in
-        + conv_taps[:, 1:2] * (padded_in[:, 1:-1] * same_one)
-        + conv_taps[:, 0:1] * (padded_in[:, :-2] * same_two)
-    )
-    gated_out = out_gate.astype(jnp.float32) * conv_out
-    channels = gated_out.shape[0]
-    by_head = gated_out.reshape(channels // HEAD, HEAD, -1)
-    by_head = by_head * lax.rsqrt(jnp.mean(by_head * by_head, axis=1, keepdims=True) + norm_eps)
-    head_normed = (by_head.reshape(channels, -1) * head_gain[:, None]).astype(jnp.bfloat16)
+    channels, width = out_proj.shape
     rows = resid.shape[0]
-    width = resid.shape[1]
     half = rows // 2
     slot = max(2, rows // 8)
-    sp_count = lax.axis_size("sp")
+    sp_count, tp_count = lax.axis_size("sp"), lax.axis_size("tp")
     local_experts = w_gate.shape[0]
-    whole_rows = (
+    if (
         sp_count == 4
-        and lax.axis_size("tp") % 2 == 0
+        and tp_count >= 4
+        and tp_count & (tp_count - 1) == 0
+        and channels == SUB
+        and channels % HEAD == 0
         and width % 1024 == 0
+        and rows % (2 * SUB) == 0
+        and conv_in.shape[1] == tp_count * rows
         and rows <= 2 * local_experts * slot
-    )
-    if whole_rows:
-        mine, everyone = every_column(out_proj), route_lists(route_ids, route_weight)
-        head_normed, mine, everyone = lax.optimization_barrier((head_normed, mine, everyone))
-    by_row = lax.all_to_all(head_normed, "tp", split_axis=1, concat_axis=0, tiled=True)
-    if whole_rows:
-        tables, slot_weights = route_tables(everyone, local_experts, half, slot)
-        by_row, tables, slot_weights = lax.optimization_barrier((by_row, tables, slot_weights))
-        mixed = mix(by_row, mine)
-    else:
-        mixed = lax.dot_general(
-            by_row,
-            lax.all_gather(out_proj, "tp", axis=0, tiled=True),
-            (((0,), (0,)), ((), ())),
-            preferred_element_type=jnp.float32,
-        )
-    stream = resid.astype(jnp.float32) + mixed
-    expert_in = (
-        stream * lax.rsqrt(jnp.mean(stream * stream, axis=1, keepdims=True) + norm_eps) * norm_gain
-    ).astype(jnp.bfloat16)
-    experts_total = local_experts * sp_count
-    if whole_rows:
-        near = gather_near(expert_in[:half])
-        later, near = lax.optimization_barrier((expert_in[half:], near))
+    ):
+        rows_of, later, stream, ids, weights = front(
+            conv_in,
+            in_gate,
+            out_gate,
+            doc_ids,
+            conv_taps,
+            head_gain,
+            out_proj,
+            resid,
+            norm_gain,
+            route_ids,
+            route_weight,
+        )
+        tables, slot_weights = route_tables(ids, weights, local_experts, half, slot)
         held = gather_near(later)
-        rows_of = jnp.stack(gather_far(*near))
         partials, sent = [], []
         for block_no in range(2):
             partial, held = experts_on(
@@ -248,6 +655,36 @@
             own = own + partials[block_no].astype(jnp.float32)
             totals.append(own + one.astype(jnp.float32) + two.astype(jnp.float32))
         return jnp.concatenate(totals, axis=0).astype(jnp.bfloat16)
+    gated_in = in_gate.astype(jnp.float32) * conv_in.astype(jnp.float32)
+    doc_value = doc_ids.astype(jnp.float32)
+    edge = jnp.concatenate([gated_in[:, -2:], doc_value[None, -2:]], axis=0)
+    edge = shifted(edge, "sp", 1)
+    earlier_in, earlier_doc = edge[:-1], edge[-1]
+    padded_in = jnp.concatenate([earlier_in, gated_in], axis=1)
+    padded_doc = jnp.concatenate([earlier_doc, doc_value])
+    same_one = (padded_doc[1:-1] == doc_value).astype(jnp.float32)
+    same_two = (padded_doc[:-2] == doc_value).astype(jnp.float32)
+    conv_out = (
+        conv_taps[:, 2:3] * gated_in
+        + conv_taps[:, 1:2] * (padded_in[:, 1:-1] * same_one)
+        + conv_taps[:, 0:1] * (padded_in[:, :-2] * same_two)
+    )
+    gated_out = out_gate.astype(jnp.float32) * conv_out
+    by_head = gated_out.reshape(channels // HEAD, HEAD, -1)
+    by_head = by_head * lax.rsqrt(jnp.mean(by_head * by_head, axis=1, keepdims=True) + norm_eps)
+    head_normed = (by_head.reshape(channels, -1) * head_gain[:, None]).astype(jnp.bfloat16)
+    by_row = lax.all_to_all(head_normed, "tp", split_axis=1, concat_axis=0, tiled=True)
+    mixed = lax.dot_general(
+        by_row,
+        lax.all_gather(out_proj, "tp", axis=0, tiled=True),
+        (((0,), (0,)), ((), ())),
+        preferred_element_type=jnp.float32,
+    )
+    stream = resid.astype(jnp.float32) + mixed
+    expert_in = (
+        stream * lax.rsqrt(jnp.mean(stream * stream, axis=1, keepdims=True) + norm_eps) * norm_gain
+    ).astype(jnp.bfloat16)
+    experts_total = local_experts * sp_count
     parts = []
     for block_no in range(2):
         block_ids = route_ids[block_no * half : (block_no + 1) * half]

time: 218 us -> 183 us (0.84); the launches traced: 214 us -> 183 us
  Pallas kernels: 0 us -> 71.6 us
  waiting for transfers between devices: 99.8 us -> 56.8 us
  starting transfers between devices: 43.2 us -> 15.4 us
  matrix products: 41.2 us -> 30.5 us
  local copies, waits for them, and re-layouts: 14.1 us -> 3.42 us
  other arithmetic: 15 us -> 4.96 us
    pallas_call x0 -> x1, Pallas kernels: none -> 71.6 us  [front(): pl.pallas_call(functools.partial(front_kernel, tp_count), out_shape=(jax....]
    ppermute x27 -> x16, waiting for transfers between devices: 92.4 us -> 56.8 us  [neighbour(): lax.ppermute(value, 'sp', [(source, source ^ bit) for source in range(cou...]
    all_to_all x2 -> x0, starting transfers between devices: 12 us -> none  [the longest x1 6.69 us: body(): lax.all_to_all(head_normed, 'tp', split_axis=1, concat_axis=0, tiled=True)]
    ppermute x27 -> x16, starting transfers between devices: 27.2 us -> 15.4 us  [neighbour(): lax.ppermute(value, 'sp', [(source, source ^ bit) for source in range(cou...]
    unnamed x46 -> x18, local copies, waits for them, and re-layouts: 8.38 us -> 0.58 us
    dot_general x2, matrix products: 11.5 us -> 4.69 us  [experts_on(): jnp.einsum('emf,efd->emd', hidden, w_down, preferred_element_type=jnp.flo...]
    dot_general x1 -> x0, matrix products: 5.55 us -> none  [mix(): lax.dot_general(by_row, jnp.concatenate(order, axis=1), (((0,), (0,)), ((...]
    ppermute x5 -> x0, starting transfers between devices: 3.98 us -> none  [the longest x1 3.4 us: shifted(): lax.ppermute(value, axis, [(source, source + steps) for source in range(l...]
  transfers between devices with their start and end apart: 34 -> 16, of which waited for: 17 -> 8; matrix products, arithmetic and copies ran while one was open for 26% -> 18% of each run, Pallas kernels for 0% -> 0%
where the time goes in v1:
time: 183 us
  Pallas kernels  71.6 us (39%)
  waiting for transfers between devices  56.8 us (31%)
  matrix products  30.5 us (17%)
  starting transfers between devices  15.4 us (8%)
  other arithmetic  4.96 us (3%)
  local copies, waits for them, and re-layouts  3.42 us (2%)
    pallas_call x1, Pallas kernels, front(): pl.pallas_call(functools.partial(front_kernel, tp_count), out_shape=(jax....  71.6 us
    ppermute x16, waiting for transfers between devices, neighbour(): lax.ppermute(value, 'sp', [(source, source ^ bit) for source in range(cou...  56.8 us
    ppermute x16, starting transfers between devices, neighbour(): lax.ppermute(value, 'sp', [(source, source ^ bit) for source in range(cou...  15.4 us
    dot_general x2, matrix products, experts_on(): jnp.einsum('emd,edf->emf', packed, w_up, preferred_element_type=jnp.float32)  8.5 us
    dot_general x2, matrix products, experts_on(): jnp.einsum('emd,edf->emf', packed, w_gate, preferred_element_type=jnp.flo...  8.19 us
    dot_general x2, matrix products, experts_on(): jnp.einsum('nest,ntd->ensd', table, rows, preferred_element_type=jnp.floa...  6.3 us
    dot_general x2, matrix products, experts_on(): jnp.einsum('emf,efd->emd', hidden, w_down, preferred_element_type=jnp.flo...  4.69 us
  transfers between devices with their start and end apart: 16, of which 8 were waited for; matrix products, arithmetic and copies ran while one was open for 18% of the time, Pallas kernels for 0%

profile of v1, /device:TPU:8, one launch (start us, length us, event | category | flops | bytes accessed | tf_op | source)
XLA Modules:
  0.0 183.0 jit_solution(16539457935861634275)
XLA Ops:
  0.0 71.6 %front.1 = (bf16[4,256,2048]{2,1,0:T(8,128)(2,1)}, bf16[256,2048]{1,0:T(8,128)(2,1)}, f32[512,2048]{1,0:T(8,128)}, s32[4,2,512]{2,1,0:T(2,128)}, f32[4,2,512]{2,1,0:T(2,128)}) custom-call(bf16[128,4096]{1,0:T(8,128)(2,1)} %conv_in.1, bf16[128,4096]{1,0:T(8,128)(2,1)} %in_gate.1, bf16[128,4096]{1,0:T(8,128)(2,1)} %out_gate.1, s32[1,4096]{1,0:T(1,128)} %bitcast.125, ...), custom_call_target="tpu_custom_call" | custom-call | tf_op jit(solution)/shard_map/front/pallas_call | solution.py:517
  71.6 1.3 collective-permute-start.1
  72.9 0.8 collective-permute-start
  73.7 0.7 eq.28
  74.4 0.7 broadcast_in_dim.49
  75.2 0.1 compare_reduce_fusion
  75.3 0.1 fusion.26
  75.4 0.2 fusion.19
  75.5 0.3 iota_compare_fusion
  75.8 0.4 select_reduce_fusion
  76.2 0.1 mul.39
  76.3 0.1 mul.44
  76.4 3.4 %convert_bitcast_fusion.1 = bf16[4,4,64,2048]{3,2,0,1:T(8,128)(2,1)S(1)} fusion(bf16[4,256,2048]{2,1,0:T(8,128)(2,1)} %get-tuple-element.21, pred[4,2,4,64,256]{4,3,2,0,1:T(32,128)(4,1)S(1)} %iota_compare_fusion), kind=kOutput, calls=%fused_computation.17 | convolution fusion | flops 1075838976 | bytes 8650752 | tf_op jit(solution)/shard_map/nest,ntd->ensd/dot_general | solution.py:102
  79.9 0.0 slice-start.2
  79.9 0.3 copy.36
  80.2 0.0 slice-start.3
  80.2 0.0 slice-start.4
  80.2 5.9 %fusion.28 = f32[4,256,512]{2,1,0:T(8,128)S(1)} fusion(bf16[4,256,2048]{2,1,0:T(8,128)(2,1)S(1)} %bitcast.119, bf16[4,2048,512]{2,1,0:T(8,128)(2,1)} %param.25), kind=kOutput, calls=%fused_computation.67 | convolution fusion | flops 2147483648 | bytes 14680064 | tf_op jit(solution)/shard_map/emd,edf->emf/dot_general | solution.py:104
  86.1 0.0 slice-start.5
  86.1 2.5 %multiply_convert_fusion.3 = bf16[4,256,512]{2,1,0:T(8,128)(2,1)S(1)} fusion(f32[4,256,512]{2,1,0:T(8,128)S(1)} %fusion.28, bf16[4,256,2048]{2,1,0:T(8,128)(2,1)S(1)} %bitcast.120, bf16[4,2048,512]{2,1,0:T(8,128)(2,1)S(1)} %bitcast.134), kind=kOutput, calls=%fused_computation.29 | convolution fusion | flops 2150629376 | bytes 15728640 | tf_op jit(solution)/shard_map/emd,edf->emf/dot_general | solution.py:105
  88.6 7.8 %collective-permute-done.1 = bf16[256,2048]{1,0:T(8,128)(2,1)S(1)} collective-permute-done((bf16[256,2048]{1,0:T(8,128)(2,1)}, bf16[256,2048]{1,0:T(8,128)(2,1)S(1)}, u32[]{:S(2)}, u32[]{:S(2)}) %collective-permute-start.1) | collective-permute-done | bytes 1048608 | tf_op jit(solution)/shard_map/ppermute | solution.py:46
  96.4 0.8 collective-permute-done
  97.2 1.2 collective-permute-start.3
  98.5 0.9 collective-permute-start.2
  99.3 2.3 %multiply_convert_fusion.1 = bf16[4,256,2048]{2,1,0:T(8,128)(2,1)S(1)} fusion(bf16[4,256,512]{2,1,0:T(8,128)(2,1)S(1)} %multiply_convert_fusion.3, bf16[4,512,2048]{2,1,0:T(8,128)(2,1)S(1)} %bitcast.136, f32[4,256]{1,0:T(4,128)S(1)} %mul.39), kind=kOutput, calls=%fused_computation.3 | convolution fusion | flops 2151677952 | bytes 13635584 | tf_op jit(solution)/shard_map/emf,efd->emd/dot_general | solution.py:111
  101.7 1.3 bitcast_convert_fusion.1
  103.0 0.2 slice_bitcast_fusion.14
  103.3 1.1 collective-permute-start.7
  104.3 1.0 collective-permute-start.6
  105.4 1.0 collective-permute-start.5
  106.4 5.7 %collective-permute-done.3 = bf16[128,2048]{1,0:T(8,128)(2,1)S(1)} collective-permute-done((bf16[128,2048]{1,0:T(8,128)(2,1)S(1)}, bf16[128,2048]{1,0:T(8,128)(2,1)S(1)}, u32[]{:S(2)}, u32[]{:S(2)}) %collective-permute-start.3) | collective-permute-done | bytes 524320 | tf_op jit(solution)/shard_map/ppermute | solution.py:46
  112.1 1.2 collective-permute-start.4
  113.3 0.0 collective-permute-done.2
  113.3 0.1 maximum_bitcast_fusion.4
  113.3 0.0 slice-start.1
  113.3 2.9 %convert_bitcast_fusion = bf16[4,4,64,2048]{3,2,0,1:T(8,128)(2,1)S(1)} fusion(bf16[1,256,2048]{2,1,0:T(8,128)(2,1)S(1)} %maximum_bitcast_fusion.4, bf16[1,256,2048]{2,1,0:T(8,128)(2,1)S(1)} %bitcast.123, bf16[1,256,2048]{2,1,0:T(8,128)(2,1)S(1)} %bitcast.124, bf16[1,256,2048]{2,1,0:T(8,128)(2,1)} %bitcast.139, ...), kind=kOutput, calls=%fused_computation.16 | convolution fusion | flops 1092616192 | bytes 8650752 | tf_op jit(solution)/shard_map/nest,ntd->ensd/dot_general | solution.py:102
  116.2 0.3 copy.40
  116.5 0.5 slice-done.1
  117.1 2.3 %fusion.29 = f32[4,256,512]{2,1,0:T(8,128)S(1)} fusion(bf16[4,256,2048]{2,1,0:T(8,128)(2,1)S(1)} %bitcast.121, bf16[4,2048,512]{2,1,0:T(8,128)(2,1)S(1)} %bitcast.132), kind=kOutput, calls=%fused_computation.68 | convolution fusion | flops 2147483648 | bytes 14680064 | tf_op jit(solution)/shard_map/emd,edf->emf/dot_general | solution.py:104
  119.4 0.0 slice-start.7
  119.4 6.0 %multiply_convert_fusion.2 = bf16[4,256,512]{2,1,0:T(8,128)(2,1)S(1)} fusion(f32[4,256,512]{2,1,0:T(8,128)S(1)} %fusion.29, bf16[4,256,2048]{2,1,0:T(8,128)(2,1)S(1)} %bitcast.122, bf16[4,2048,512]{2,1,0:T(8,128)(2,1)} %param.26), kind=kOutput, calls=%fused_computation.27 | convolution fusion | flops 2150629376 | bytes 15728640 | tf_op jit(solution)/shard_map/emd,edf->emf/dot_general | solution.py:105
  125.5 2.3 %multiply_convert_fusion = bf16[4,256,2048]{2,1,0:T(8,128)(2,1)S(1)} fusion(bf16[4,256,512]{2,1,0:T(8,128)(2,1)S(1)} %multiply_convert_fusion.2, bf16[4,512,2048]{2,1,0:T(8,128)(2,1)S(1)} %bitcast.138, f32[4,256]{1,0:T(4,128)S(1)} %mul.44), kind=kOutput, calls=%fused_computation.2 | convolution fusion | flops 2151677952 | bytes 13635584 | tf_op jit(solution)/shard_map/emf,efd->emd/dot_general | solution.py:111
  127.8 0.0 collective-permute-done.6
  127.8 0.4 fusion.22
  128.2 4.7 %collective-permute-done.5 = bf16[128,2048]{1,0:T(8,128)(2,1)S(1)} collective-permute-done((bf16[128,2048]{1,0:T(8,128)(2,1)S(1)}, bf16[128,2048]{1,0:T(8,128)(2,1)S(1)}, u32[]{:S(2)}, u32[]{:S(2)}) %collective-permute-start.5) | collective-permute-done | bytes 524320 | tf_op jit(solution)/shard_map/ppermute | solution.py:46
  133.0 1.3 bitcast_convert_fusion
  134.3 0.2 slice_bitcast_fusion.9
  134.5 0.6 collective-permute-start.13
  135.2 1.1 collective-permute-start.11
  136.3 0.9 collective-permute-start.8
  137.2 1.5 collective-permute-start.9
  138.7 0.6 collective-permute-start.15
  139.2 10.2 %collective-permute-done.13 = bf16[128,2048]{1,0:T(8,128)(2,1)S(1)} collective-permute-done((bf16[128,2048]{1,0:T(8,128)(2,1)S(1)}, bf16[128,2048]{1,0:T(8,128)(2,1)S(1)}, u32[]{:S(2)}, u32[]{:S(2)}) %collective-permute-start.13) | collective-permute-done | bytes 524320 | tf_op jit(solution)/shard_map/ppermute | solution.py:46
  149.4 0.6 collective-permute-start.10
  150.0 0.0 collective-permute-done.11
  150.0 0.4 fusion.20
  150.4 1.2 collective-permute-start.14
  151.6 9.1 %collective-permute-done.8 = bf16[128,2048]{1,0:T(8,128)(2,1)S(1)} collective-permute-done((bf16[128,2048]{1,0:T(8,128)(2,1)S(1)}, bf16[128,2048]{1,0:T(8,128)(2,1)S(1)}, u32[]{:S(2)}, u32[]{:S(2)}) %collective-permute-start.8) | collective-permute-done | bytes 524320 | tf_op jit(solution)/shard_map/ppermute | solution.py:46
  160.6 0.6 collective-permute-start.12
  161.2 0.0 collective-permute-done.9
  161.2 11.2 %collective-permute-done.15 = bf16[128,2048]{1,0:T(8,128)(2,1)S(1)} collective-permute-done((bf16[128,2048]{1,0:T(8,128)(2,1)S(1)}, bf16[128,2048]{1,0:T(8,128)(2,1)S(1)}, u32[]{:S(2)}, u32[]{:S(2)}) %collective-permute-start.15) | collective-permute-done | bytes 524320 | tf_op jit(solution)/shard_map/ppermute | solution.py:46
  172.4 7.3 %collective-permute-done.14 = bf16[128,2048]{1,0:T(8,128)(2,1)S(1)} collective-permute-done((bf16[128,2048]{1,0:T(8,128)(2,1)S(1)}, bf16[128,2048]{1,0:T(8,128)(2,1)S(1)}, u32[]{:S(2)}, u32[]{:S(2)}) %collective-permute-start.14) | collective-permute-done | bytes 524320 | tf_op jit(solution)/shard_map/ppermute | solution.py:46
  179.8 1.7 fusion.18
  181.5 1.5 pad_maximum_fusion
  (25 shorter events, 0.1 us)
Async XLA Ops:
  71.6 24.8 %collective-permute-start.1 = (bf16[256,2048]{1,0:T(8,128)(2,1)}, bf16[256,2048]{1,0:T(8,128)(2,1)S(1)}, u32[]{:S(2)}, u32[]{:S(2)}) collective-permute-start(bf16[256,2048]{1,0:T(8,128)(2,1)} %get-tuple-element.25), channel_id=1, source_target_pairs={{0,16},{8,24},{16,0},{24,8},{1,17},{9,25},{17,1},{25,9},{2,18},{10... | collective-permute-start | bytes 3145736 | tf_op jit(solution)/shard_map/ppermute | solution.py:46
  72.9 24.3 %collective-permute-start = (bf16[256,2048]{1,0:T(8,128)(2,1)}, bf16[256,2048]{1,0:T(8,128)(2,1)S(1)}, u32[]{:S(2)}, u32[]{:S(2)}) collective-permute-start(bf16[256,2048]{1,0:T(8,128)(2,1)} %get-tuple-element.25), channel_id=1, source_target_pairs={{0,8},{8,0},{16,24},{24,16},{1,9},{9,1},{17,25},{25,17},{2,10},{10... | collective-permute-start | bytes 3145736 | tf_op jit(solution)/shard_map/ppermute | solution.py:46
  79.9 6.2 %slice-start.2 = ((s8[8388608]{0:T(1024)(128)(4,1)}), s8[4194304]{0:T(1024)(128)(4,1)S(1)}, s32[]{:S(2)}) async-start(s8[8388608]{0:T(1024)(128)(4,1)} %bitcast.133), calls=%async_computation.2 | async-start | bytes 8388608
  80.2 5.9 %slice-start.3 = ((s8[8388608]{0:T(1024)(128)(4,1)}), s8[4194304]{0:T(1024)(128)(4,1)S(1)}, s32[]{:S(2)}) async-start(s8[8388608]{0:T(1024)(128)(4,1)} %bitcast.133), calls=%async_computation.3 | async-start | bytes 8388608
  80.2 19.1 %slice-start.4 = ((s8[8388608]{0:T(1024)(128)(4,1)}), s8[4194304]{0:T(1024)(128)(4,1)S(1)}, s32[]{:S(2)}) async-start(s8[8388608]{0:T(1024)(128)(4,1)} %bitcast.135), calls=%async_computation.4 | async-start | bytes 8388608
  86.1 13.2 %slice-start.5 = ((s8[8388608]{0:T(1024)(128)(4,1)}), s8[4194304]{0:T(1024)(128)(4,1)S(1)}, s32[]{:S(2)}) async-start(s8[8388608]{0:T(1024)(128)(4,1)} %bitcast.135), calls=%async_computation.5 | async-start | bytes 8388608
  97.2 14.9 %collective-permute-start.3 = (bf16[128,2048]{1,0:T(8,128)(2,1)S(1)}, bf16[128,2048]{1,0:T(8,128)(2,1)S(1)}, u32[]{:S(2)}, u32[]{:S(2)}) collective-permute-start(bf16[128,2048]{1,0:T(8,128)(2,1)S(1)} %slice.117), channel_id=1, source_target_pairs={{0,8},{8,0},{16,24},{24,16},{1,9},{9,1},{17,25},{25,17},{2,10},{10... | collective-permute-start | bytes 1572872 | tf_op jit(solution)/shard_map/ppermute | solution.py:46
  98.5 14.8 %collective-permute-start.2 = (bf16[128,2048]{1,0:T(8,128)(2,1)S(1)}, bf16[128,2048]{1,0:T(8,128)(2,1)S(1)}, u32[]{:S(2)}, u32[]{:S(2)}) collective-permute-start(bf16[128,2048]{1,0:T(8,128)(2,1)S(1)} %slice.116), channel_id=1, source_target_pairs={{0,16},{8,24},{16,0},{24,8},{1,17},{9,25},{17,1},{25,9},{2,18},{10... | collective-permute-start | bytes 1572872 | tf_op jit(solution)/shard_map/ppermute | solution.py:46
  103.3 24.5 %collective-permute-start.7 = (bf16[128,2048]{1,0:T(8,128)(2,1)S(1)}, bf16[128,2048]{1,0:T(8,128)(2,1)S(1)}, u32[]{:S(2)}, u32[]{:S(2)}) collective-permute-start(bf16[128,2048]{1,0:T(8,128)(2,1)S(1)} %get-tuple-element.43), channel_id=1, source_target_pairs={{0,8},{8,0},{16,24},{24,16},{1,9},{9,1},{17,25},{25,17},{2,10},{10... | collective-permute-start | bytes 1572872 | tf_op jit(solution)/shard_map/ppermute | solution.py:46
  104.3 23.5 %collective-permute-start.6 = (bf16[128,2048]{1,0:T(8,128)(2,1)S(1)}, bf16[128,2048]{1,0:T(8,128)(2,1)S(1)}, u32[]{:S(2)}, u32[]{:S(2)}) collective-permute-start(bf16[128,2048]{1,0:T(8,128)(2,1)S(1)} %get-tuple-element.44), channel_id=1, source_target_pairs={{0,16},{8,24},{16,0},{24,8},{1,17},{9,25},{17,1},{25,9},{2,18},{10... | collective-permute-start | bytes 1572872 | tf_op jit(solution)/shard_map/ppermute | solution.py:46
  105.4 27.6 %collective-permute-start.5 = (bf16[128,2048]{1,0:T(8,128)(2,1)S(1)}, bf16[128,2048]{1,0:T(8,128)(2,1)S(1)}, u32[]{:S(2)}, u32[]{:S(2)}) collective-permute-start(bf16[128,2048]{1,0:T(8,128)(2,1)S(1)} %get-tuple-element.45), channel_id=1, source_target_pairs={{0,16},{8,24},{16,0},{24,8},{1,17},{9,25},{17,1},{25,9},{2,18},{10... | collective-permute-start | bytes 1572872 | tf_op jit(solution)/shard_map/ppermute | solution.py:46
  112.1 20.9 %collective-permute-start.4 = (bf16[128,2048]{1,0:T(8,128)(2,1)S(1)}, bf16[128,2048]{1,0:T(8,128)(2,1)S(1)}, u32[]{:S(2)}, u32[]{:S(2)}) collective-permute-start(bf16[128,2048]{1,0:T(8,128)(2,1)S(1)} %get-tuple-element.46), channel_id=1, source_target_pairs={{0,8},{8,0},{16,24},{24,16},{1,9},{9,1},{17,25},{25,17},{2,10},{10... | collective-permute-start | bytes 1572872 | tf_op jit(solution)/shard_map/ppermute | solution.py:46
  113.3 3.3 %slice-start = ((s8[8388608]{0:T(1024)(128)(4,1)}), s8[4194304]{0:T(1024)(128)(4,1)S(1)}, s32[]{:S(2)}) async-start(s8[8388608]{0:T(1024)(128)(4,1)} %bitcast.131), calls=%async_computation | async-start | bytes 8388608
  113.3 3.7 %slice-start.1 = ((s8[8388608]{0:T(1024)(128)(4,1)}), s8[4194304]{0:T(1024)(128)(4,1)S(1)}, s32[]{:S(2)}) async-start(s8[8388608]{0:T(1024)(128)(4,1)} %bitcast.131), calls=%async_computation.1 | async-start | bytes 8388608
  117.1 8.4 %slice-start.6 = ((s8[8388608]{0:T(1024)(128)(4,1)}), s8[4194304]{0:T(1024)(128)(4,1)S(1)}, s32[]{:S(2)}) async-start(s8[8388608]{0:T(1024)(128)(4,1)} %bitcast.137), calls=%async_computation.6 | async-start | bytes 8388608
  119.4 6.1 %slice-start.7 = ((s8[8388608]{0:T(1024)(128)(4,1)}), s8[4194304]{0:T(1024)(128)(4,1)S(1)}, s32[]{:S(2)}) async-start(s8[8388608]{0:T(1024)(128)(4,1)} %bitcast.137), calls=%async_computation.7 | async-start | bytes 8388608
  134.3 45.5 %copy-start = (f32[512,2048]{1,0:T(8,128)S(1)}, f32[512,2048]{1,0:T(8,128)}, u32[]{:S(2)}) copy-start(f32[512,2048]{1,0:T(8,128)} %get-tuple-element.19) | copy-start | bytes 12582916
  134.5 14.9 %collective-permute-start.13 = (bf16[128,2048]{1,0:T(8,128)(2,1)S(1)}, bf16[128,2048]{1,0:T(8,128)(2,1)S(1)}, u32[]{:S(2)}, u32[]{:S(2)}) collective-permute-start(bf16[128,2048]{1,0:T(8,128)(2,1)S(1)} %get-tuple-element.37), channel_id=1, source_target_pairs={{0,8},{8,0},{16,24},{24,16},{1,9},{9,1},{17,25},{25,17},{2,10},{10... | collective-permute-start | bytes 1572872 | tf_op jit(solution)/shard_map/ppermute | solution.py:46
  135.2 14.8 %collective-permute-start.11 = (bf16[128,2048]{1,0:T(8,128)(2,1)S(1)}, bf16[128,2048]{1,0:T(8,128)(2,1)S(1)}, u32[]{:S(2)}, u32[]{:S(2)}) collective-permute-start(bf16[128,2048]{1,0:T(8,128)(2,1)S(1)} %get-tuple-element.39), channel_id=1, source_target_pairs={{0,16},{8,24},{16,0},{24,8},{1,17},{9,25},{17,1},{25,9},{2,18},{10... | collective-permute-start | bytes 1572872 | tf_op jit(solution)/shard_map/ppermute | solution.py:46
  136.3 24.3 %collective-permute-start.8 = (bf16[128,2048]{1,0:T(8,128)(2,1)S(1)}, bf16[128,2048]{1,0:T(8,128)(2,1)S(1)}, u32[]{:S(2)}, u32[]{:S(2)}) collective-permute-start(bf16[128,2048]{1,0:T(8,128)(2,1)S(1)} %get-tuple-element.29), channel_id=1, source_target_pairs={{0,8},{8,0},{16,24},{24,16},{1,9},{9,1},{17,25},{25,17},{2,10},{10... | collective-permute-start | bytes 1572872 | tf_op jit(solution)/shard_map/ppermute | solution.py:46
  137.2 24.0 %collective-permute-start.9 = (bf16[128,2048]{1,0:T(8,128)(2,1)S(1)}, bf16[128,2048]{1,0:T(8,128)(2,1)S(1)}, u32[]{:S(2)}, u32[]{:S(2)}) collective-permute-start(bf16[128,2048]{1,0:T(8,128)(2,1)S(1)} %get-tuple-element.30), channel_id=1, source_target_pairs={{0,16},{8,24},{16,0},{24,8},{1,17},{9,25},{17,1},{25,9},{2,18},{10... | collective-permute-start | bytes 1572872 | tf_op jit(solution)/shard_map/ppermute | solution.py:46
  138.7 33.8 %collective-permute-start.15 = (bf16[128,2048]{1,0:T(8,128)(2,1)S(1)}, bf16[128,2048]{1,0:T(8,128)(2,1)S(1)}, u32[]{:S(2)}, u32[]{:S(2)}) collective-permute-start(bf16[128,2048]{1,0:T(8,128)(2,1)S(1)} %get-tuple-element.38), channel_id=1, source_target_pairs={{0,16},{8,24},{16,0},{24,8},{1,17},{9,25},{17,1},{25,9},{2,18},{10... | collective-permute-start | bytes 1572872 | tf_op jit(solution)/shard_map/ppermute | solution.py:46
  149.4 23.0 %collective-permute-start.10 = (bf16[128,2048]{1,0:T(8,128)(2,1)S(1)}, bf16[128,2048]{1,0:T(8,128)(2,1)S(1)}, u32[]{:S(2)}, u32[]{:S(2)}) collective-permute-start(bf16[128,2048]{1,0:T(8,128)(2,1)S(1)} %get-tuple-element.40), channel_id=1, source_target_pairs={{0,8},{8,0},{16,24},{24,16},{1,9},{9,1},{17,25},{25,17},{2,10},{10... | collective-permute-start | bytes 1572872 | tf_op jit(solution)/shard_map/ppermute | solution.py:46
  150.4 29.4 %collective-permute-start.14 = (bf16[128,2048]{1,0:T(8,128)(2,1)S(1)}, bf16[128,2048]{1,0:T(8,128)(2,1)S(1)}, u32[]{:S(2)}, u32[]{:S(2)}) collective-permute-start(bf16[128,2048]{1,0:T(8,128)(2,1)S(1)} %get-tuple-element.35), channel_id=1, source_target_pairs={{0,16},{8,24},{16,0},{24,8},{1,17},{9,25},{17,1},{25,9},{2,18},{10... | collective-permute-start | bytes 1572872 | tf_op jit(solution)/shard_map/ppermute | solution.py:46
  160.6 19.1 %collective-permute-start.12 = (bf16[128,2048]{1,0:T(8,128)(2,1)S(1)}, bf16[128,2048]{1,0:T(8,128)(2,1)S(1)}, u32[]{:S(2)}, u32[]{:S(2)}) collective-permute-start(bf16[128,2048]{1,0:T(8,128)(2,1)S(1)} %get-tuple-element.36), channel_id=1, source_target_pairs={{0,8},{8,0},{16,24},{24,16},{1,9},{9,1},{17,25},{25,17},{2,10},{10... | collective-permute-start | bytes 1572872 | tf_op jit(solution)/shard_map/ppermute | solution.py:46

commit v2 on v1

--- a/solution.py
+++ b/solution.py
@@ -39,82 +39,6 @@
             places[:, choice_k]
         ].astype(jnp.float32)
     return totals
-
-
-def neighbour(value, bit):
-    count = lax.axis_size("sp")
-    return lax.ppermute(value, "sp", [(source, source ^ bit) for source in range(count)])
-
-
-def gather_near(value):
-    return value, neighbour(value, 1), neighbour(value, 2)
-
-
-def gather_far(value, from_one, from_two):
-    middle = value.shape[0] // 2
-    low = neighbour(from_one[:middle], 2)
-    high = neighbour(from_two[middle:], 1)
-    return [value, from_one, from_two, jnp.concatenate([low, high], axis=0)]
-
-
-def scatter_four(parts):
-    middle = parts[3].shape[0] // 2
-    low = neighbour(parts[3][:middle], 1)
-    high = neighbour(parts[3][middle:], 2)
-    straight = neighbour(parts[1][:middle], 1), neighbour(parts[2][middle:], 2)
-    return straight, (add(parts[1][middle:], high), add(parts[2][:middle], low))
-
-
-def scatter_rest(straight, joined):
-    one = jnp.concatenate([straight[0], neighbour(joined[0], 1)], axis=0)
-    two = jnp.concatenate([neighbour(joined[1], 2), straight[1]], axis=0)
-    return one, two
-
-
-def add(left, right):
-    return (left.astype(jnp.float32) + right.astype(jnp.float32)).astype(jnp.bfloat16)
-
-
-def route_tables(ids, weights, local_experts, half, slot):
-    me = lax.axis_index("sp")
-    top = ids.shape[1]
-    ids = ids.reshape(4, top, -1, half)
-    weights = weights.reshape(4, top, -1, half)
-    experts = me * local_experts + jnp.arange(local_experts, dtype=jnp.int32)
-    hit = ids[:, :, :, None, :] == experts[None, None, None, :, None]
-    marks = jnp.any(hit, axis=1)
-    weight_of = jnp.sum(jnp.where(hit, weights[:, :, :, None], 0.0), axis=1)
-    earlier = (
-        jnp.arange(half)[:, None] < jnp.arange(half)[None, :]
-    ).astype(jnp.bfloat16)
-    rank = jnp.dot(
-        marks.astype(jnp.bfloat16).reshape(-1, half), earlier, preferred_element_type=jnp.float32
-    ).reshape(marks.shape)
-    rank = jnp.where(marks, rank.astype(jnp.int32), -1)
-    chosen = rank[:, :, :, None, :] == jnp.arange(slot, dtype=jnp.int32)[None, None, None, :, None]
-    slot_weight = jnp.sum(jnp.where(chosen, weight_of[:, :, :, None, :], 0.0), axis=4)
-    return chosen.astype(jnp.bfloat16), slot_weight
-
-
-def experts_on(rows, table, slot_weight, w_gate, w_up, w_down, held, late):
-    sources, local_experts, slot, half = table.shape
-    width = rows.shape[2]
-    packed = jnp.einsum("nest,ntd->ensd", table, rows, preferred_element_type=jnp.float32)
-    packed = packed.astype(jnp.bfloat16).reshape(local_experts, sources * slot, width)
-    gate_part = jnp.einsum("emd,edf->emf", packed, w_gate, preferred_element_type=jnp.float32)
-    up_part = jnp.einsum("emd,edf->emf", packed, w_up, preferred_element_type=jnp.float32)
-    hidden = (jax.nn.silu(gate_part) * up_part).astype(jnp.bfloat16)
-    if late:
-        hidden = lax.optimization_barrier(hidden)
-    else:
-        hidden, held = lax.optimization_barrier((hidden, held))
-    down = jnp.einsum("emf,efd->emd", hidden, w_down, preferred_element_type=jnp.float32)
-    scale = jnp.transpose(slot_weight, (1, 0, 2)).reshape(local_experts, sources * slot, 1)
-    down = (down * scale).astype(jnp.bfloat16).reshape(local_experts, sources, slot, width)
-    if late:
-        down, held = lax.optimization_barrier((down, held))
-    total = jnp.einsum("nest,ensd->ntd", table, down, preferred_element_type=jnp.float32)
-    return total.astype(jnp.bfloat16), held
 
 
 MESH = pl.DeviceIdType.MESH
@@ -134,9 +58,11 @@
     norm_gain_in,
     ids,
     weights,
-    rows_out,
-    later_out,
-    stream_out,
+    w_gate,
+    w_up,
+    w_down,
+    out_low,
+    out_high,
     ids_out,
     weights_out,
     in_buf,
@@ -152,10 +78,21 @@
     outgoing,
     by_row,
     gathered,
-    later,
     stream,
+    gate_now,
+    up_now,
+    down_now,
+    marks,
+    share,
+    rank,
+    table,
+    slot_weight,
+    packed,
+    hidden,
+    partial,
+    inbox,
+    back,
     local_sem,
-    out_sem,
     edge_send,
     edge_recv,
     list_send,
@@ -174,6 +111,13 @@
     near_recv,
     far_send,
     far_recv,
+    weight_sem,
+    first_send,
+    first_recv,
+    straight_send,
+    straight_recv,
+    merged_send,
+    merged_recv,
 ):
     sp, tp = lax.axis_index("sp"), lax.axis_index("tp")
     z, core = tp // 2, tp % 2
@@ -360,11 +304,12 @@
         region = proj.at[block_rows(step), columns(diagonal, core)]
         send(region, region, core_send.at[3, step], core_recv.at[3, step], sp, tp ^ 1)
 
-    def others_done(step):
-        other = 1 - core
-        for k, place in enumerate((sp, near_of[0], near_of[1], diagonal)):
+    places = (sp, near_of[0], near_of[1], diagonal)
+
+    def other_half(k):
+        for step in range(1, planes):
             arrive(
-                proj.at[block_rows(step), columns(place, other)],
+                proj.at[block_rows(step), columns(places[k], 1 - core)],
                 core_send.at[k, step],
                 core_recv.at[k, step],
             )
@@ -380,22 +325,294 @@
         lax.fori_loop(0, tp_count - 1, one, 0)
         by_row[q, :, my_channels] = piece(tp, q)
 
-    for q in range(1, subs):
+    for q in (1, 2):
         convolve(q)
     for step in range(1, planes):
-        if step == planes - 1:
-            for copy in slices:
-                copy.wait_send()
-            start_trade(order[0])
         spread_slice(step)
+        if step == 1:
+            for at, target in enumerate((in_buf, gate_buf, doc_buf)):
+                arrive(target.at[:, edge], edge_send.at[at], edge_recv.at[at])
+            doc_buf[:, edge] = jnp.where(sp == 0, -1, doc_buf[:, edge])
+            convolve(0)
+    for copy in slices:
+        copy.wait_send()
+    start_trade(order[0])
     for step in range(1, planes):
         spread_plane(step)
-    for at, target in enumerate((in_buf, gate_buf, doc_buf)):
-        arrive(target.at[:, edge], edge_send.at[at], edge_recv.at[at])
-    doc_buf[:, edge] = jnp.where(sp == 0, -1, doc_buf[:, edge])
-    convolve(0)
-    for step in range(1, planes):
-        spread_corner(step)
+
+    tile = width // 4
+    local_experts, _, hidden_width = w_gate.shape
+    slot = table.shape[2] // local_experts
+
+    def load_weights(at):
+        side, expert = at % 2, at % local_experts
+        return [
+            pltpu.make_async_copy(source.at[expert], target.at[side], weight_sem.at[k, side])
+            for k, (source, target) in enumerate(
+                ((w_gate, gate_now), (w_up, up_now), (w_down, down_now))
+            )
+        ]
+
+    for at in range(2):
+        for copy in load_weights(at):
+            copy.start()
+
+    def make_tables():
+        for d in range(1, 4):
+            arrive(ids_out.at[d], list_send.at[0, d], list_recv.at[0, d])
+            arrive(weights_out.at[d], list_send.at[1, d], list_recv.at[1, d])
+        deep = marks.shape[2]
+        line = lax.broadcasted_iota(jnp.int32, (deep, half), 0)
+        experts = sp * local_experts + line
+        ahead = (
+            lax.broadcasted_iota(jnp.int32, (half, half), 0)
+            < lax.broadcasted_iota(jnp.int32, (half, half), 1)
+        ).astype(jnp.bfloat16)
+        for b in range(2):
+            for n in range(4):
+                hits, amount = jnp.zeros((deep, half)), jnp.zeros((deep, half))
+                for k in range(ids.shape[0]):
+                    here = pl.ds(b * half, half)
+                    hit = (ids_out[n, pl.ds(k, 1), here] == experts) & (line < local_experts)
+                    hits = hits + hit.astype(jnp.float32)
+                    amount = amount + jnp.where(hit, weights_out[n, pl.ds(k, 1), here], 0.0)
+                marks[b, n] = hits
+                share[b, n] = amount
+            flat = marks[b].reshape(4 * deep, half)
+            order_of = jnp.dot(flat.astype(jnp.bfloat16), ahead, preferred_element_type=jnp.float32)
+            rank[b] = jnp.where(flat > 0, order_of, -1.0).reshape(4, deep, half)
+
+            def fill(n, carry, b=b):
+                spots = lax.broadcasted_iota(jnp.int32, (slot, half), 0).astype(jnp.float32)
+                for e in range(local_experts):
+                    chosen = rank[b, n, pl.ds(e, 1), :] == spots
+                    table[b, n, pl.ds(e * slot, slot), :] = chosen.astype(jnp.float32).astype(
+                        jnp.bfloat16
+                    )
+                    total = jnp.sum(
+                        jnp.where(chosen, share[b, n, pl.ds(e, 1), :], 0.0), axis=1, keepdims=True
+                    )
+                    slot_weight[b, e, pl.ds(pl.multiple_of(n * slot, slot), slot), :] = (
+                        jnp.broadcast_to(total, (slot, slot_weight.shape[3]))
+                    )
+                return carry
+
+            lax.fori_loop(0, 4, fill, 0)
+
+    def near_region(place, q):
+        return gathered.at[q // first, place, pl.ds(q % first * SUB, SUB)]
+
+    def far_region(q, k):
+        return gathered.at[q // first, 3, pl.ds(q % first * SUB + k * (SUB // 2), SUB // 2)]
+
+    def got_rows(q):
+        def got(d, carry):
+            theirs = pl.ds(pl.multiple_of((tp ^ d) * channels, channels), channels)
+            arrive(by_row.at[q, :, theirs], trade_send.at[q, d], trade_recv.at[q, d])
+            return carry
+
+        lax.fori_loop(1, tp_count, got, 0)
+
+    def project_tile(q, place):
+        mine = pl.ds(q * SUB, SUB)
+        cols = pl.ds(pl.multiple_of(place * tile, tile), tile)
+        value = resid_buf[mine, cols].astype(jnp.float32) + jnp.dot(
+            by_row[q], proj[:, cols], preferred_element_type=jnp.float32
+        )
+        stream[mine, cols] = value
+        return jnp.sum(value * value, axis=1, keepdims=True)
+
+    def normalize_rows(q, total):
+        mine = pl.ds(q * SUB, SUB)
+        there = pl.ds(q % first * SUB, SUB)
+        scale = lax.rsqrt(total / width + norm_eps)
+
+        def normalize(n, carry):
+            cols = pl.ds(pl.multiple_of(n * tile, tile), tile)
+            value = (stream[mine, cols] * scale * norm_gain[:, cols]).astype(jnp.bfloat16)
+            gathered[q // first, 0, there, cols] = value
+            return carry
+
+        lax.fori_loop(0, 4, normalize, 0)
+
+    def project_rows(q):
+        got_rows(q)
+        total = lax.fori_loop(
+            0, 4, lambda n, total: total + project_tile(q, n), jnp.zeros((SUB, 1), jnp.float32)
+        )
+        normalize_rows(q, total)
+
+    def spread_rows(q):
+        for k in range(2):
+            send(
+                near_region(0, q),
+                near_region(1 + k, q),
+                near_send.at[k, q],
+                near_recv.at[k, q],
+                near_of[k],
+                tp,
+            )
+
+    far_copies = []
+
+    def relay_rows(q):
+        for k in range(2):
+            arrive(near_region(1 + k, q), near_send.at[k, q], near_recv.at[k, q])
+            part = gathered.at[
+                q // first, 1 + k, pl.ds(q % first * SUB + k * (SUB // 2), SUB // 2)
+            ]
+            copy = remote(
+                part, far_region(q, k), far_send.at[k, q], far_recv.at[k, q], near_of[1 - k], tp
+            )
+            copy.start()
+            far_copies.append(copy)
+
+    def far_rows(q):
+        for k in range(2):
+            arrive(far_region(q, k), far_send.at[k, q], far_recv.at[k, q])
+
+    def run_experts(b, between=None):
+        def pack(at, carry):
+            n, cols = at // 4, pl.ds(pl.multiple_of(at % 4 * tile, tile), tile)
+            rows_in = jnp.dot(
+                table[b, n], gathered[b, n, :, cols], preferred_element_type=jnp.float32
+            ).astype(jnp.bfloat16)
+            for e in range(local_experts):
+                packed[e, pl.ds(pl.multiple_of(n * slot, slot), slot), cols] = rows_in[
+                    e * slot : (e + 1) * slot
+                ]
+            return carry
+
+        lax.fori_loop(0, 16, pack, 0)
+
+        def expert(e, carry):
+            at = b * local_experts + e
+            side = at % 2
+            for copy in load_weights(at):
+                copy.wait()
+            piece_width = hidden_width // 2
+
+            def up(c, carry):
+                cols = pl.ds(pl.multiple_of(c * piece_width, piece_width), piece_width)
+                gate = jnp.dot(
+                    packed[e], gate_now[side, :, cols], preferred_element_type=jnp.float32
+                )
+                value = jnp.dot(
+                    packed[e], up_now[side, :, cols], preferred_element_type=jnp.float32
+                )
+                hidden[:, cols] = (gate / (1.0 + jnp.exp(-gate)) * value).astype(jnp.bfloat16)
+                return carry
+
+            lax.fori_loop(0, 2, up, 0)
+
+            def down(c, carry):
+                cols = pl.ds(pl.multiple_of(c * tile, tile), tile)
+                value = jnp.dot(
+                    hidden[...], down_now[side, :, cols], preferred_element_type=jnp.float32
+                )
+                packed[e, :, cols] = (value * slot_weight[b, e, :, 0:1]).astype(jnp.bfloat16)
+                return carry
+
+            lax.fori_loop(0, 4, down, 0)
+
+            @pl.when(at + 2 < 2 * local_experts)
+            def _():
+                for copy in load_weights(at + 2):
+                    copy.start()
+
+            return carry
+
+        middle = local_experts if between is None else local_experts // 2
+        lax.fori_loop(0, middle, expert, 0)
+        if between is not None:
+            between()
+            lax.fori_loop(middle, local_experts, expert, 0)
+
+    def combine(b, n):
+        def one(c, carry):
+            cols = pl.ds(pl.multiple_of(c * tile, tile), tile)
+            pieces = jnp.concatenate(
+                [packed[e, pl.ds(n * slot, slot), cols] for e in range(local_experts)], axis=0
+            )
+            partial[b, n, :, cols] = lax.dot_general(
+                table[b, n], pieces, (((0,), (0,)), ((), ())), preferred_element_type=jnp.float32
+            ).astype(jnp.bfloat16)
+            return carry
+
+        lax.fori_loop(0, 4, one, 0)
+
+    part_of = [pl.ds(k * (half // 2), half // 2) for k in range(2)]
+
+    def send_first(b):
+        copies = []
+        for k in range(2):
+            copy = remote(
+                partial.at[b, 3, part_of[k]],
+                inbox.at[b, k],
+                first_send.at[b, k],
+                first_recv.at[b, k],
+                near_of[k],
+                tp,
+            )
+            copy.start()
+            copies.append(copy)
+        return copies
+
+    def send_straight(b):
+        for k in range(2):
+            send(
+                partial.at[b, 1 + k, part_of[k]],
+                back.at[b, k, part_of[k]],
+                straight_send.at[b, k],
+                straight_recv.at[b, k],
+                near_of[k],
+                tp,
+            )
+
+    strip = 16
+
+    def merge(b):
+        for k in range(2):
+            arrive(inbox.at[b, k], first_send.at[b, k], first_recv.at[b, k])
+
+            def add(at, carry, k=k):
+                there = pl.ds(pl.multiple_of(k * (half // 2) + at * strip, strip), strip)
+                here = pl.ds(pl.multiple_of(at * strip, strip), strip)
+                partial[b, 2 - k, there, :] = (
+                    partial[b, 2 - k, there, :].astype(jnp.float32)
+                    + inbox[b, k, here, :].astype(jnp.float32)
+                ).astype(jnp.bfloat16)
+                return carry
+
+            lax.fori_loop(0, half // 2 // strip, add, 0)
+            send(
+                partial.at[b, 2 - k, part_of[k]],
+                back.at[b, 1 - k, part_of[k]],
+                merged_send.at[b, k],
+                merged_recv.at[b, k],
+                near_of[1 - k],
+                tp,
+            )
+
+    def finish(b):
+        for k in range(2):
+            arrive(back.at[b, k, part_of[k]], straight_send.at[b, k], straight_recv.at[b, k])
+        for k in range(2):
+            arrive(back.at[b, 1 - k, part_of[k]], merged_send.at[b, k], merged_recv.at[b, k])
+
+            def add(at, carry, k=k):
+                here = pl.ds(pl.multiple_of(k * (half // 2) + at * strip, strip), strip)
+                there = pl.ds(pl.multiple_of(b * half + k * (half // 2) + at * strip, strip), strip)
+                value = stream[there, :] + partial[b, 0, here, :].astype(jnp.float32)
+                value = value + back[b, 0, here, :].astype(jnp.float32)
+                (out_low, out_high)[b][here, :] = (
+                    value + back[b, 1, here, :].astype(jnp.float32)
+                ).astype(jnp.bfloat16)
+                return carry
+
+            lax.fori_loop(0, half // 2 // strip, add, 0)
+
+    got_rows(order[0])
     sent_trade(order[0])
     start_trade(order[1])
     for copy in loads[6:]:
@@ -405,104 +622,71 @@
         slice_send.at[1],
         slice_recv.at[1],
     )
-    for step in range(1, planes):
-        others_done(step)
-
-    tile = width // 4
-    stores = []
-    for at_q, q in enumerate(order):
-        if at_q > 0:
-            sent_trade(q)
-            if at_q + 1 < subs:
-                start_trade(order[at_q + 1])
-
-        def got(d, carry, q=q):
-            theirs = pl.ds(pl.multiple_of((tp ^ d) * channels, channels), channels)
-            arrive(by_row.at[q, :, theirs], trade_send.at[q, d], trade_recv.at[q, d])
-            return carry
-
-        lax.fori_loop(1, tp_count, got, 0)
-        mine = pl.ds(q * SUB, SUB)
-
-        def project(n, total, q=q, mine=mine):
-            cols = pl.ds(pl.multiple_of(n * tile, tile), tile)
-            value = resid_buf[mine, cols].astype(jnp.float32) + jnp.dot(
-                by_row[q], proj[:, cols], preferred_element_type=jnp.float32
-            )
-            stream[mine, cols] = value
-            return total + jnp.sum(value * value, axis=1, keepdims=True)
-
-        total = lax.fori_loop(0, 4, project, jnp.zeros((SUB, 1), jnp.float32))
-        scale = lax.rsqrt(total / width + norm_eps)
-
-        def normalize(n, carry, q=q, mine=mine, scale=scale):
-            cols = pl.ds(pl.multiple_of(n * tile, tile), tile)
-            value = (stream[mine, cols] * scale * norm_gain[:, cols]).astype(jnp.bfloat16)
-            if q < first:
-                gathered[0, mine, cols] = value
-            else:
-                later[pl.ds((q - first) * SUB, SUB), cols] = value
-            return carry
-
-        lax.fori_loop(0, 4, normalize, 0)
-        if q < first:
-            region = gathered.at[0, mine]
-            for k in range(2):
-                send(
-                    region,
-                    gathered.at[1 + k, mine],
-                    near_send.at[k, q],
-                    near_recv.at[k, q],
-                    near_of[k],
-                    tp,
-                )
-    stores.append(pltpu.make_async_copy(stream, stream_out, out_sem.at[0]))
-    stores.append(pltpu.make_async_copy(later, later_out, out_sem.at[1]))
-    stores.append(pltpu.make_async_copy(gathered.at[0], rows_out.at[0], out_sem.at[2]))
-    for copy in stores:
-        copy.start()
-    for d in range(1, 4):
-        arrive(ids_out.at[d], list_send.at[0, d], list_recv.at[0, d])
-        arrive(weights_out.at[d], list_send.at[1, d], list_recv.at[1, d])
-
-    for q in range(first):
-        for k in range(2):
-            arrive(
-                gathered.at[1 + k, pl.ds(q * SUB, SUB)], near_send.at[k, q], near_recv.at[k, q]
-            )
-            part = pl.ds(q * SUB + k * (SUB // 2), SUB // 2)
-            send(
-                gathered.at[1 + k, part],
-                gathered.at[3, part],
-                far_send.at[k, q],
-                far_recv.at[k, q],
-                near_of[1 - k],
-                tp,
-            )
-    for k in range(2):
-        store = pltpu.make_async_copy(gathered.at[1 + k], rows_out.at[1 + k], out_sem.at[3 + k])
-        store.start()
-        stores.append(store)
-    for q in range(first):
-        for k in range(2):
-            part = pl.ds(q * SUB + k * (SUB // 2), SUB // 2)
-            arrive(gathered.at[3, part], far_send.at[k, q], far_recv.at[k, q])
-        store = pltpu.make_async_copy(
-            gathered.at[3, pl.ds(q * SUB, SUB)],
-            rows_out.at[3, pl.ds(q * SUB, SUB)],
-            out_sem.at[5 + q],
-        )
-        store.start()
-        stores.append(store)
-    for copy in stores:
-        copy.wait()
+    total = jnp.zeros((SUB, 1), jnp.float32)
+    for k in range(4):
+        if k == 3:
+            for step in range(1, planes):
+                spread_corner(step)
+        other_half(k)
+        total = total + project_tile(order[0], places[k])
+    normalize_rows(order[0], total)
+    spread_rows(order[0])
+    make_tables()
+    for q in range(3, subs):
+        convolve(q)
+    for at_q in range(1, first):
+        sent_trade(order[at_q])
+        if at_q + 1 < subs:
+            start_trade(order[at_q + 1])
+        project_rows(order[at_q])
+        spread_rows(order[at_q])
+    for at_q in range(first):
+        relay_rows(order[at_q])
+        late = order[first + at_q]
+        sent_trade(late)
+        if first + at_q + 1 < subs:
+            start_trade(order[first + at_q + 1])
+        project_rows(late)
+    for copy in far_copies[:2]:
+        copy.wait_send()
+    spread_rows(order[first])
+    for at_q in range(first):
+        far_rows(order[at_q])
+    for at_q in range(1, first):
+        spread_rows(order[first + at_q])
+    run_experts(0, lambda: relay_rows(order[first]))
+    for at_q in range(1, first):
+        relay_rows(order[first + at_q])
+    combine(0, 3)
+    firsts = send_first(0)
+    combine(0, 1)
+    combine(0, 2)
+    send_straight(0)
+    combine(0, 0)
+    merge(0)
+    for at_q in range(first):
+        far_rows(order[first + at_q])
+    run_experts(1)
+    combine(1, 3)
+    firsts_two = send_first(1)
+    combine(1, 1)
+    combine(1, 2)
+    combine(1, 0)
+    for copy in firsts_two:
+        copy.wait_send()
+    send_straight(1)
+    finish(0)
+    merge(1)
+    finish(1)
+    for copy in firsts + far_copies[2:]:
+        copy.wait_send()
     for copy in pending:
         copy.wait_send()
 
 
 def front(
     conv_in, in_gate, out_gate, doc_ids, conv_taps, head_gain, out_proj, resid, norm_gain,
-    route_ids, route_weight,
+    route_ids, route_weight, w_gate, w_up, w_down,
 ):
     tp_count = lax.axis_size("tp")
     channels, width = out_proj.shape
@@ -511,21 +695,18 @@
     half, subs = rows // 2, rows // SUB
     first, planes = half // SUB, tp_count // 2
     top = route_ids.shape[1]
+    local_experts, _, hidden_width = w_gate.shape
+    slot = max(2, rows // 8)
     hbm = pl.BlockSpec(memory_space=pltpu.HBM)
-    vmem = pl.BlockSpec(memory_space=pltpu.VMEM)
     dma = pltpu.SemaphoreType.DMA
     return pl.pallas_call(
         functools.partial(front_kernel, tp_count),
-        out_shape=(
-            jax.ShapeDtypeStruct((4, half, width), jnp.bfloat16),
-            jax.ShapeDtypeStruct((half, width), jnp.bfloat16),
-            jax.ShapeDtypeStruct((rows, width), jnp.float32),
-            jax.ShapeDtypeStruct((4, top, rows), jnp.int32),
-            jax.ShapeDtypeStruct((4, top, rows), jnp.float32),
-        ),
-        in_specs=[hbm] * 11,
-        out_specs=(hbm, hbm, hbm, vmem, vmem),
+        out_shape=[pltpu.VMEM((half, width), jnp.bfloat16)] * 2,
+        in_specs=[hbm] * 14,
+        out_specs=[pl.BlockSpec(memory_space=pltpu.VMEM)] * 2,
         scratch_shapes=[
+            pltpu.VMEM((4, top, rows), jnp.int32),
+            pltpu.VMEM((4, top, rows), jnp.float32),
             pltpu.VMEM((channels, SUB + positions), jnp.bfloat16),
             pltpu.VMEM((channels, SUB + positions), jnp.bfloat16),
             pltpu.VMEM((channels, positions), jnp.bfloat16),
@@ -538,11 +719,22 @@
             pltpu.VMEM((4, channels, SUB), jnp.float32),
             pltpu.VMEM((subs, tp_count, SUB, channels), jnp.bfloat16),
             pltpu.VMEM((subs, SUB, tp_count * channels), jnp.bfloat16),
-            pltpu.VMEM((4, half, width), jnp.bfloat16),
-            pltpu.VMEM((half, width), jnp.bfloat16),
+            pltpu.VMEM((2, 4, half, width), jnp.bfloat16),
             pltpu.VMEM((rows, width), jnp.float32),
+            pltpu.VMEM((2, width, hidden_width), jnp.bfloat16),
+            pltpu.VMEM((2, width, hidden_width), jnp.bfloat16),
+            pltpu.VMEM((2, hidden_width, width), jnp.bfloat16),
+            pltpu.VMEM((2, 4, 8, half), jnp.float32),
+            pltpu.VMEM((2, 4, 8, half), jnp.float32),
+            pltpu.VMEM((2, 4, 8, half), jnp.float32),
+            pltpu.VMEM((2, 4, local_experts * slot, half), jnp.bfloat16),
+            pltpu.VMEM((2, local_experts, 4 * slot, 128), jnp.float32),
+            pltpu.VMEM((local_experts, 4 * slot, width), jnp.bfloat16),
+            pltpu.VMEM((4 * slot, hidden_width), jnp.bfloat16),
+            pltpu.VMEM((2, 4, half, width), jnp.bfloat16),
+            pltpu.VMEM((2, 2, half // 2, width), jnp.bfloat16),
+            pltpu.VMEM((2, 2, half, width), jnp.bfloat16),
             dma((11,)),
-            dma((5 + first,)),
             dma((3,)),
             dma((3,)),
             dma((2, 4)),
@@ -557,13 +749,20 @@
             dma((4, planes)),
             dma((subs, tp_count)),
             dma((subs, tp_count)),
-            dma((2, first)),
-            dma((2, first)),
-            dma((2, first)),
-            dma((2, first)),
+            dma((2, subs)),
+            dma((2, subs)),
+            dma((2, subs)),
+            dma((2, subs)),
+            dma((3, 2)),
+            dma((2, 2)),
+            dma((2, 2)),
+            dma((2, 2)),
+            dma((2, 2)),
+            dma((2, 2)),
+            dma((2, 2)),
         ],
         compiler_params=pltpu.CompilerParams(
-            collective_id=0, has_side_effects=True, vmem_limit_bytes=60 * 1024 * 1024
+            collective_id=0, has_side_effects=True, vmem_limit_bytes=59944 * 1024
         ),
         name="front",
     )(
@@ -578,6 +777,9 @@
         norm_gain[None],
         route_ids.T,
         route_weight.T,
+        w_gate,
+        w_up,
+        w_down,
     )
 
 
@@ -614,7 +816,7 @@
         and conv_in.shape[1] == tp_count * rows
         and rows <= 2 * local_experts * slot
     ):
-        rows_of, later, stream, ids, weights = front(
+        halves = front(
             conv_in,
             in_gate,
             out_gate,
@@ -626,35 +828,11 @@
             norm_gain,
             route_ids,
             route_weight,
-        )
-        tables, slot_weights = route_tables(ids, weights, local_experts, half, slot)
-        held = gather_near(later)
-        partials, sent = [], []
-        for block_no in range(2):
-            partial, held = experts_on(
-                rows_of,
-                tables[:, block_no],
-                slot_weights[:, block_no],
-                w_gate,
-                w_up,
-                w_down,
-                held,
-                block_no > 0,
-            )
-            if block_no == 0:
-                rows_of = jnp.stack(gather_far(*held))
-            else:
-                sent.append(scatter_rest(*held))
-            partials.append(partial[0])
-            held = scatter_four([partial[distance] for distance in range(4)])
-        sent.append(scatter_rest(*held))
-        totals = []
-        for block_no in range(2):
-            one, two = sent[block_no]
-            own = stream[block_no * half : (block_no + 1) * half]
-            own = own + partials[block_no].astype(jnp.float32)
-            totals.append(own + one.astype(jnp.float32) + two.astype(jnp.float32))
-        return jnp.concatenate(totals, axis=0).astype(jnp.bfloat16)
+            w_gate,
+            w_up,
+            w_down,
+        )
+        return jnp.concatenate(halves, axis=0)
     gated_in = in_gate.astype(jnp.float32) * conv_in.astype(jnp.float32)
     doc_value = doc_ids.astype(jnp.float32)
     edge = jnp.concatenate([gated_in[:, -2:], doc_value[None, -2:]], axis=0)

time: 183 us -> 171 us (0.934); the launches traced: 183 us -> 169 us
  Pallas kernels: 71.6 us -> 167 us
  waiting for transfers between devices: 56.8 us -> 0 us
  matrix products: 30.5 us -> 0 us
  starting transfers between devices: 15.4 us -> 0 us
  other arithmetic: 4.96 us -> 1.46 us
  local copies, waits for them, and re-layouts: 3.42 us -> 0 us
    pallas_call x1, Pallas kernels: 71.6 us -> 167 us  [front(): pl.pallas_call(functools.partial(front_kernel, tp_count), out_shape=[pltp...]
    ppermute x16 -> x0, waiting for transfers between devices: 56.8 us -> none  [neighbour(): lax.ppermute(value, 'sp', [(source, source ^ bit) for source in range(cou...]
    dot_general x11 -> x0, matrix products: 30.5 us -> none  [the longest x2 8.5 us: experts_on(): jnp.einsum('emd,edf->emf', packed, w_up, preferred_element_type=jnp.float32)]
    ppermute x16 -> x0, starting transfers between devices: 15.4 us -> none  [neighbour(): lax.ppermute(value, 'sp', [(source, source ^ bit) for source in range(cou...]
  transfers between devices with their start and end apart: 16 -> 0, of which waited for: 8 -> 0; matrix products, arithmetic and copies ran while one was open for 18% -> 0% of each run, Pallas kernels for 0% -> 0%
where the time goes in v2:
time: 171 us; the launch traced here: 169 us
  Pallas kernels  167 us (98%)
    pallas_call x1, Pallas kernels, front(): pl.pallas_call(functools.partial(front_kernel, tp_count), out_shape=[pltp...  167 us

profile of v2, /device:TPU:8, one launch (start us, length us, event | category | flops | bytes accessed | tf_op | source)
XLA Modules:
  0.0 168.6 jit_solution(9499523303874242289)
XLA Ops:
  0.0 167.2 %front.1 = (bf16[256,2048]{1,0:T(8,128)(2,1)S(1)}, bf16[256,2048]{1,0:T(8,128)(2,1)S(1)}) custom-call(bf16[128,4096]{1,0:T(8,128)(2,1)} %conv_in.1, bf16[128,4096]{1,0:T(8,128)(2,1)} %in_gate.1, bf16[128,4096]{1,0:T(8,128)(2,1)} %out_gate.1, s32[1,4096]{1,0:T(1,128)} %bitcast.6, f32[3,128]{1,0:T(4,128)} %bitcast.10, f32[1,128]{1,0:T(1,128)} %bitcast.11, ...), custom_call_target="tpu_custom_call" | custom-call | tf_op jit(solution)/shard_map/front/pallas_call | solution.py:702
  167.2 1.5 pad_maximum_fusion

commit v3 on v2

--- a/solution.py
+++ b/solution.py
@@ -43,6 +43,7 @@
 
 MESH = pl.DeviceIdType.MESH
 SUB = 128
+EARLY = 64
 
 
 def front_kernel(
@@ -92,6 +93,8 @@
     partial,
     inbox,
     back,
+    early_resid,
+    early_normed,
     local_sem,
     edge_send,
     edge_recv,
@@ -114,10 +117,13 @@
     weight_sem,
     first_send,
     first_recv,
-    straight_send,
+    back_send,
     straight_recv,
-    merged_send,
     merged_recv,
+    resid_send,
+    resid_recv,
+    normed_send,
+    normed_recv,
 ):
     sp, tp = lax.axis_index("sp"), lax.axis_index("tp")
     z, core = tp // 2, tp % 2
@@ -128,7 +134,6 @@
     planes = tp_count // 2
     near_of = [sp ^ 1, sp ^ 2]
     diagonal = sp ^ 3
-    pending = []
 
     def remote(source, target, send_sem, recv_sem, to_sp, to_tp):
         return pltpu.make_async_remote_copy(
@@ -141,12 +146,13 @@
         )
 
     def send(source, target, send_sem, recv_sem, to_sp, to_tp):
-        copy = remote(source, target, send_sem, recv_sem, to_sp, to_tp)
-        copy.start()
-        pending.append(copy)
-
-    def arrive(region, send_sem, recv_sem):
-        remote(region, region, send_sem, recv_sem, near_of[0], tp).wait_recv()
+        remote(source, target, send_sem, recv_sem, to_sp, to_tp).start()
+
+    def left(region, send_sem):
+        remote(region, region, send_sem, send_sem, near_of[0], tp).wait_send()
+
+    def arrive(region, recv_sem):
+        remote(region, region, recv_sem, recv_sem, near_of[0], tp).wait_recv()
 
     tail = conv_in.shape[1] - SUB
     loads = [
@@ -194,23 +200,35 @@
         return pl.ds(pl.multiple_of(place * (2 * eighth) + side * eighth, eighth), eighth)
 
     my_rows = pl.ds(pl.multiple_of(tp * channels, channels), channels)
+    early = EARLY
     slices = []
     for d in range(2, tp_count):
         side = core ^ (d & 1)
         copy = remote(
             out_proj.at[:, columns(sp, side)],
             proj.at[my_rows, columns(sp, side)],
-            slice_send.at[d],
-            slice_recv.at[d],
+            slice_send.at[1],
+            slice_recv.at[d // 2],
             sp,
             tp ^ d,
         )
+        slices.append(copy)
+
+    for copy in slices:
         copy.start()
-        slices.append(copy)
-    send(out_proj, proj.at[my_rows], slice_send.at[1], slice_recv.at[1], sp, tp ^ 1)
+    for k in range(2):
+        send(
+            resid.at[pl.ds(rows - early, early)],
+            early_resid.at[k],
+            resid_send.at[0],
+            resid_recv.at[0],
+            near_of[k],
+            tp,
+        )
+    send(out_proj, proj.at[my_rows], slice_send.at[0], slice_recv.at[0], sp, tp ^ 1)
     for d in range(1, 4):
-        send(ids, ids_out.at[d], list_send.at[0, d], list_recv.at[0, d], sp ^ d, tp)
-        send(weights, weights_out.at[d], list_send.at[1, d], list_recv.at[1, d], sp ^ d, tp)
+        send(ids, ids_out.at[d], list_send.at[0], list_recv.at[0], sp ^ d, tp)
+        send(weights, weights_out.at[d], list_send.at[1], list_recv.at[1], sp ^ d, tp)
     for copy in loads[:6]:
         copy.wait()
     for k in range(3):
@@ -243,8 +261,8 @@
         return remote(
             outgoing.at[q, d],
             by_row.at[q, :, my_channels],
-            trade_send.at[q, d],
-            trade_recv.at[q, d],
+            trade_send.at[q],
+            trade_recv.at[q],
             sp,
             tp ^ d,
         )
@@ -257,11 +275,7 @@
         lax.fori_loop(0, tp_count - 1, begin, 0)
 
     def sent_trade(q):
-        def sent(d, carry):
-            trade(q, d).wait_send()
-            return carry
-
-        lax.fori_loop(1, tp_count, sent, 0)
+        left(outgoing.at[q, pl.ds(1, tp_count - 1)], trade_send.at[q])
 
     def block_rows(step):
         deep = 2 * channels
@@ -272,37 +286,24 @@
         return pl.ds(pl.multiple_of((z ^ step) * deep + upper * channels, channels), channels)
 
     def spread_slice(step):
-        arrive_rows = [
-            pl.ds(pl.multiple_of((tp ^ (2 * step + odd)) * channels, channels), channels)
-            for odd in range(2)
-        ]
-        for odd in range(2):
-            d = 2 * step + odd
-            arrive(
-                proj.at[arrive_rows[odd], columns(sp, core)], slice_send.at[d], slice_recv.at[d]
-            )
         region = proj.at[block_rows(step), columns(sp, core)]
+        arrive(region, slice_recv.at[step])
         for k in range(2):
-            send(region, region, plane_send.at[k, step], plane_recv.at[k, step], near_of[k], tp)
-        send(region, region, core_send.at[0, step], core_recv.at[0, step], sp, tp ^ 1)
+            send(region, region, plane_send.at[0], plane_recv.at[k, step - 1], near_of[k], tp)
+        send(region, region, core_send.at[0], core_recv.at[0, step - 1], sp, tp ^ 1)
 
     def spread_plane(step):
         for k in range(2):
             region = proj.at[block_rows(step), columns(near_of[k], core)]
-            arrive(region, plane_send.at[k, step], plane_recv.at[k, step])
+            arrive(region, plane_recv.at[k, step - 1])
             part = proj.at[part_rows(step, k), columns(near_of[k], core)]
-            send(part, part, corner_send.at[k, step], corner_recv.at[k, step], near_of[1 - k], tp)
-            send(region, region, core_send.at[1 + k, step], core_recv.at[1 + k, step], sp, tp ^ 1)
+            send(part, part, corner_send.at[0], corner_recv.at[step - 1], near_of[1 - k], tp)
+            send(region, region, core_send.at[0], core_recv.at[1 + k, step - 1], sp, tp ^ 1)
 
     def spread_corner(step):
-        for k in range(2):
-            arrive(
-                proj.at[part_rows(step, k), columns(diagonal, core)],
-                corner_send.at[k, step],
-                corner_recv.at[k, step],
-            )
         region = proj.at[block_rows(step), columns(diagonal, core)]
-        send(region, region, core_send.at[3, step], core_recv.at[3, step], sp, tp ^ 1)
+        arrive(region, corner_recv.at[step - 1])
+        send(region, region, core_send.at[0], core_recv.at[3, step - 1], sp, tp ^ 1)
 
     places = (sp, near_of[0], near_of[1], diagonal)
 
@@ -310,8 +311,7 @@
         for step in range(1, planes):
             arrive(
                 proj.at[block_rows(step), columns(places[k], 1 - core)],
-                core_send.at[k, step],
-                core_recv.at[k, step],
+                core_recv.at[k, step - 1],
             )
 
     order = [1, 0, *range(2, subs)]
@@ -325,19 +325,19 @@
         lax.fori_loop(0, tp_count - 1, one, 0)
         by_row[q, :, my_channels] = piece(tp, q)
 
-    for q in (1, 2):
-        convolve(q)
-    for step in range(1, planes):
+    convolve(1)
+    convolve(2)
+    steps = list(range(1, planes))
+    for at, step in enumerate(steps):
         spread_slice(step)
-        if step == 1:
-            for at, target in enumerate((in_buf, gate_buf, doc_buf)):
-                arrive(target.at[:, edge], edge_send.at[at], edge_recv.at[at])
+        if at == 0:
+            for k, target in enumerate((in_buf, gate_buf, doc_buf)):
+                arrive(target.at[:, edge], edge_recv.at[k])
             doc_buf[:, edge] = jnp.where(sp == 0, -1, doc_buf[:, edge])
             convolve(0)
-    for copy in slices:
-        copy.wait_send()
+    left(proj.at[pl.ds(0, 2 * (planes - 1) * channels // 8)], slice_send.at[1])
     start_trade(order[0])
-    for step in range(1, planes):
+    for step in steps:
         spread_plane(step)
 
     tile = width // 4
@@ -358,9 +358,8 @@
             copy.start()
 
     def make_tables():
-        for d in range(1, 4):
-            arrive(ids_out.at[d], list_send.at[0, d], list_recv.at[0, d])
-            arrive(weights_out.at[d], list_send.at[1, d], list_recv.at[1, d])
+        arrive(ids_out.at[pl.ds(1, 3)], list_recv.at[0])
+        arrive(weights_out.at[pl.ds(1, 3)], list_recv.at[1])
         deep = marks.shape[2]
         line = lax.broadcasted_iota(jnp.int32, (deep, half), 0)
         experts = sp * local_experts + line
@@ -399,19 +398,63 @@
 
             lax.fori_loop(0, 4, fill, 0)
 
+    def early_region(place, k):
+        part = pl.ds(half - early + k * (early // 2), early // 2)
+        return gathered.at[1, place, part]
+
+    def project_early():
+        arrive(early_resid, resid_recv.at[0])
+        arrive(early_normed, normed_recv.at[0])
+        deep = 2 * early
+
+        def stream_of(n):
+            cols = pl.ds(pl.multiple_of(n * tile, tile), tile)
+            value = early_resid[:, :, cols].astype(jnp.float32).reshape(deep, tile)
+            return cols, value + jnp.dot(
+                early_normed[...].reshape(deep, tp_count * channels),
+                proj[:, cols],
+                preferred_element_type=jnp.float32,
+            )
+
+        def project(n, total):
+            value = stream_of(n)[1]
+            return total + jnp.sum(value * value, axis=1, keepdims=True)
+
+        total = lax.fori_loop(0, 4, project, jnp.zeros((deep, 1), jnp.float32))
+        scale = lax.rsqrt(total / width + norm_eps)
+
+        def normalize(n, carry):
+            cols, value = stream_of(n)
+            value = (value * scale * norm_gain[:, cols]).astype(jnp.bfloat16)
+            for k in range(2):
+                gathered[1, 1 + k, pl.ds(half - early, early), cols] = value[
+                    k * early : (k + 1) * early
+                ]
+            return carry
+
+        lax.fori_loop(0, 4, normalize, 0)
+        for k in range(2):
+            send(
+                early_region(1 + k, k),
+                early_region(3, k),
+                normed_send.at[1],
+                normed_recv.at[1],
+                near_of[1 - k],
+                tp,
+            )
+
+    def span(q):
+        return SUB - early if q == subs - 1 else SUB
+
     def near_region(place, q):
-        return gathered.at[q // first, place, pl.ds(q % first * SUB, SUB)]
-
-    def far_region(q, k):
-        return gathered.at[q // first, 3, pl.ds(q % first * SUB + k * (SUB // 2), SUB // 2)]
+        return gathered.at[q // first, place, pl.ds(q % first * SUB, span(q))]
+
+    def far_region(q, k, place=3):
+        part = span(q) // 2
+        return gathered.at[q // first, place, pl.ds(q % first * SUB + k * part, part)]
 
     def got_rows(q):
-        def got(d, carry):
-            theirs = pl.ds(pl.multiple_of((tp ^ d) * channels, channels), channels)
-            arrive(by_row.at[q, :, theirs], trade_send.at[q, d], trade_recv.at[q, d])
-            return carry
-
-        lax.fori_loop(1, tp_count, got, 0)
+        arrive(by_row.at[q, :, pl.ds(0, (tp_count - 1) * channels)], trade_recv.at[q])
 
     def project_tile(q, place):
         mine = pl.ds(q * SUB, SUB)
@@ -447,29 +490,26 @@
             send(
                 near_region(0, q),
                 near_region(1 + k, q),
-                near_send.at[k, q],
+                near_send.at[q],
                 near_recv.at[k, q],
                 near_of[k],
                 tp,
             )
 
-    far_copies = []
-
     def relay_rows(q):
         for k in range(2):
-            arrive(near_region(1 + k, q), near_send.at[k, q], near_recv.at[k, q])
-            part = gathered.at[
-                q // first, 1 + k, pl.ds(q % first * SUB + k * (SUB // 2), SUB // 2)
-            ]
-            copy = remote(
-                part, far_region(q, k), far_send.at[k, q], far_recv.at[k, q], near_of[1 - k], tp
+            arrive(near_region(1 + k, q), near_recv.at[k, q])
+            send(
+                far_region(q, k, 1 + k),
+                far_region(q, k),
+                far_send.at[q],
+                far_recv.at[q],
+                near_of[1 - k],
+                tp,
             )
-            copy.start()
-            far_copies.append(copy)
 
     def far_rows(q):
-        for k in range(2):
-            arrive(far_region(q, k), far_send.at[k, q], far_recv.at[k, q])
+        arrive(near_region(3, q), far_recv.at[q])
 
     def run_experts(b, between=None):
         def pack(at, carry):
@@ -544,26 +584,22 @@
     part_of = [pl.ds(k * (half // 2), half // 2) for k in range(2)]
 
     def send_first(b):
-        copies = []
         for k in range(2):
-            copy = remote(
+            send(
                 partial.at[b, 3, part_of[k]],
                 inbox.at[b, k],
-                first_send.at[b, k],
+                first_send.at[b],
                 first_recv.at[b, k],
                 near_of[k],
                 tp,
             )
-            copy.start()
-            copies.append(copy)
-        return copies
 
     def send_straight(b):
         for k in range(2):
             send(
                 partial.at[b, 1 + k, part_of[k]],
                 back.at[b, k, part_of[k]],
-                straight_send.at[b, k],
+                back_send.at[b],
                 straight_recv.at[b, k],
                 near_of[k],
                 tp,
@@ -573,7 +609,7 @@
 
     def merge(b):
         for k in range(2):
-            arrive(inbox.at[b, k], first_send.at[b, k], first_recv.at[b, k])
+            arrive(inbox.at[b, k], first_recv.at[b, k])
 
             def add(at, carry, k=k):
                 there = pl.ds(pl.multiple_of(k * (half // 2) + at * strip, strip), strip)
@@ -588,7 +624,7 @@
             send(
                 partial.at[b, 2 - k, part_of[k]],
                 back.at[b, 1 - k, part_of[k]],
-                merged_send.at[b, k],
+                back_send.at[b],
                 merged_recv.at[b, k],
                 near_of[1 - k],
                 tp,
@@ -596,9 +632,9 @@
 
     def finish(b):
         for k in range(2):
-            arrive(back.at[b, k, part_of[k]], straight_send.at[b, k], straight_recv.at[b, k])
+            arrive(back.at[b, k, part_of[k]], straight_recv.at[b, k])
         for k in range(2):
-            arrive(back.at[b, 1 - k, part_of[k]], merged_send.at[b, k], merged_recv.at[b, k])
+            arrive(back.at[b, 1 - k, part_of[k]], merged_recv.at[b, k])
 
             def add(at, carry, k=k):
                 here = pl.ds(pl.multiple_of(k * (half // 2) + at * strip, strip), strip)
@@ -619,13 +655,12 @@
         copy.wait()
     arrive(
         proj.at[pl.ds(pl.multiple_of((tp ^ 1) * channels, channels), channels)],
-        slice_send.at[1],
-        slice_recv.at[1],
+        slice_recv.at[0],
     )
     total = jnp.zeros((SUB, 1), jnp.float32)
     for k in range(4):
         if k == 3:
-            for step in range(1, planes):
+            for step in steps:
                 spread_corner(step)
         other_half(k)
         total = total + project_tile(order[0], places[k])
@@ -647,18 +682,27 @@
         if first + at_q + 1 < subs:
             start_trade(order[first + at_q + 1])
         project_rows(late)
-    for copy in far_copies[:2]:
-        copy.wait_send()
+    left(near_region(0, order[0]), far_send.at[order[0]])
     spread_rows(order[first])
     for at_q in range(first):
         far_rows(order[at_q])
     for at_q in range(1, first):
         spread_rows(order[first + at_q])
+    for k in range(2):
+        send(
+            by_row.at[subs - 1, pl.ds(SUB - early, early)],
+            early_normed.at[k],
+            normed_send.at[0],
+            normed_recv.at[0],
+            near_of[k],
+            tp,
+        )
     run_experts(0, lambda: relay_rows(order[first]))
+    combine(0, 3)
+    send_first(0)
     for at_q in range(1, first):
         relay_rows(order[first + at_q])
-    combine(0, 3)
-    firsts = send_first(0)
+    project_early()
     combine(0, 1)
     combine(0, 2)
     send_straight(0)
@@ -666,22 +710,39 @@
     merge(0)
     for at_q in range(first):
         far_rows(order[first + at_q])
+    arrive(gathered.at[1, 3, pl.ds(half - early, early)], normed_recv.at[1])
     run_experts(1)
     combine(1, 3)
-    firsts_two = send_first(1)
+    send_first(1)
     combine(1, 1)
     combine(1, 2)
     combine(1, 0)
-    for copy in firsts_two:
-        copy.wait_send()
+    left(partial.at[1, 3], first_send.at[1])
     send_straight(1)
     finish(0)
     merge(1)
     finish(1)
-    for copy in firsts + far_copies[2:]:
-        copy.wait_send()
-    for copy in pending:
-        copy.wait_send()
+    for at, target in enumerate((in_buf, gate_buf, doc_buf)):
+        left(target.at[:, edge], edge_send.at[at])
+    left(ids_out.at[pl.ds(1, 3)], list_send.at[0])
+    left(weights_out.at[pl.ds(1, 3)], list_send.at[1])
+    left(proj.at[my_rows], slice_send.at[0])
+    left(proj.at[pl.ds(0, (planes - 1) * channels // 2)], plane_send.at[0])
+    left(proj.at[pl.ds(0, (planes - 1) * channels // 4)], corner_send.at[0])
+    left(proj.at[pl.ds(0, (planes - 1) * channels)], core_send.at[0])
+    left(early_resid, resid_send.at[0])
+    left(early_normed, normed_send.at[0])
+    left(gathered.at[1, 3, pl.ds(half - early, early)], normed_send.at[1])
+    for q in range(subs):
+        left(
+            gathered.at[q // first, pl.ds(0, 2), pl.ds(q % first * SUB, span(q))],
+            near_send.at[q],
+        )
+        if q != order[0]:
+            left(near_region(0, q), far_send.at[q])
+    left(partial.at[0, 3], first_send.at[0])
+    for b in range(2):
+        left(back.at[b], back_send.at[b])
 
 
 def front(
@@ -734,32 +795,37 @@
             pltpu.VMEM((2, 4, half, width), jnp.bfloat16),
             pltpu.VMEM((2, 2, half // 2, width), jnp.bfloat16),
             pltpu.VMEM((2, 2, half, width), jnp.bfloat16),
+            pltpu.VMEM((2, EARLY, width), jnp.bfloat16),
+            pltpu.VMEM((2, EARLY, tp_count * channels), jnp.bfloat16),
             dma((11,)),
             dma((3,)),
             dma((3,)),
-            dma((2, 4)),
-            dma((2, 4)),
-            dma((tp_count,)),
-            dma((tp_count,)),
-            dma((2, planes)),
-            dma((2, planes)),
-            dma((2, planes)),
-            dma((2, planes)),
-            dma((4, planes)),
-            dma((4, planes)),
-            dma((subs, tp_count)),
-            dma((subs, tp_count)),
+            dma((2,)),
+            dma((2,)),
+            dma((2,)),
+            dma((planes,)),
+            dma((1,)),
+            dma((2, planes - 1)),
+            dma((1,)),
+            dma((planes - 1,)),
+            dma((1,)),
+            dma((4, planes - 1)),
+            dma((subs,)),
+            dma((subs,)),
+            dma((subs,)),
             dma((2, subs)),
-            dma((2, subs)),
-            dma((2, subs)),
-            dma((2, subs)),
+            dma((subs,)),
+            dma((subs,)),
             dma((3, 2)),
+            dma((2,)),
+            dma((2, 2)),
+            dma((2,)),
             dma((2, 2)),
             dma((2, 2)),
-            dma((2, 2)),
-            dma((2, 2)),
-            dma((2, 2)),
-            dma((2, 2)),
+            dma((1,)),
+            dma((1,)),
+            dma((2,)),
+            dma((2,)),
         ],
         compiler_params=pltpu.CompilerParams(
             collective_id=0, has_side_effects=True, vmem_limit_bytes=59944 * 1024

time: 171 us -> 167 us (0.977)
  Pallas kernels: 167 us -> 163 us
    pallas_call x1, Pallas kernels: 167 us -> 163 us  [front(): pl.pallas_call(functools.partial(front_kernel, tp_count), out_shape=[pltp...]
where the time goes in v3:
time: 167 us; the launch traced here: 165 us
  Pallas kernels  163 us (98%)
    pallas_call x1, Pallas kernels, front(): pl.pallas_call(functools.partial(front_kernel, tp_count), out_shape=[pltp...  163 us

profile of v3, /device:TPU:8, one launch (start us, length us, event | category | flops | bytes accessed | tf_op | source)
XLA Modules:
  0.0 164.9 jit_solution(7005881920907519448)
XLA Ops:
  0.0 163.5 %front.1 = (bf16[256,2048]{1,0:T(8,128)(2,1)S(1)}, bf16[256,2048]{1,0:T(8,128)(2,1)S(1)}) custom-call(bf16[128,4096]{1,0:T(8,128)(2,1)} %conv_in.1, bf16[128,4096]{1,0:T(8,128)(2,1)} %in_gate.1, bf16[128,4096]{1,0:T(8,128)(2,1)} %out_gate.1, s32[1,4096]{1,0:T(1,128)} %bitcast.6, f32[3,128]{1,0:T(4,128)} %bitcast.10, f32[1,128]{1,0:T(1,128)} %bitcast.11, ...), custom_call_target="tpu_custom_call" | custom-call | tf_op jit(solution)/shard_map/front/pallas_call | solution.py:763
  163.5 1.5 pad_maximum_fusion

commit v4 on v3

--- a/solution.py
+++ b/solution.py
@@ -95,6 +95,7 @@
     back,
     early_resid,
     early_normed,
+    scales,
     local_sem,
     edge_send,
     edge_recv,
@@ -124,6 +125,8 @@
     resid_recv,
     normed_send,
     normed_recv,
+    scale_send,
+    scale_recv,
 ):
     sp, tp = lax.axis_index("sp"), lax.axis_index("tp")
     z, core = tp // 2, tp % 2
@@ -326,18 +329,15 @@
         by_row[q, :, my_channels] = piece(tp, q)
 
     convolve(1)
-    convolve(2)
-    steps = list(range(1, planes))
-    for at, step in enumerate(steps):
+    for step in range(1, planes):
         spread_slice(step)
-        if at == 0:
-            for k, target in enumerate((in_buf, gate_buf, doc_buf)):
-                arrive(target.at[:, edge], edge_recv.at[k])
-            doc_buf[:, edge] = jnp.where(sp == 0, -1, doc_buf[:, edge])
-            convolve(0)
     left(proj.at[pl.ds(0, 2 * (planes - 1) * channels // 8)], slice_send.at[1])
     start_trade(order[0])
-    for step in steps:
+    for k, target in enumerate((in_buf, gate_buf, doc_buf)):
+        arrive(target.at[:, edge], edge_recv.at[k])
+    doc_buf[:, edge] = jnp.where(sp == 0, -1, doc_buf[:, edge])
+    convolve(0)
+    for step in range(1, planes):
         spread_plane(step)
 
     tile = width // 4
@@ -485,6 +485,47 @@
         )
         normalize_rows(q, total)
 
+    def spread_tile(q, place):
+        cols = pl.ds(pl.multiple_of(place * tile, tile), tile)
+        there = pl.ds(q % first * SUB, SUB)
+        value = stream[pl.ds(q * SUB, SUB), cols] * norm_gain[:, cols]
+        gathered[q // first, 0, there, cols] = value.astype(jnp.bfloat16)
+        for k in range(2):
+            send(
+                gathered.at[q // first, 0, there, cols],
+                gathered.at[q // first, 1 + k, there, cols],
+                near_send.at[q],
+                near_recv.at[k, q],
+                near_of[k],
+                tp,
+            )
+
+    def send_scales(total):
+        scale = jnp.broadcast_to(lax.rsqrt(total / width + norm_eps), (SUB, SUB))
+        scales[0] = scale.T[:8]
+        for d in range(1, 4):
+            send(scales.at[0], scales.at[d], scale_send.at[0], scale_recv.at[0], sp ^ d, tp)
+
+    def place_scales():
+        arrive(scales.at[pl.ds(1, 3)], scale_recv.at[0])
+
+        def fill(n, carry):
+            ones = jnp.ones((1, SUB), jnp.float32)
+            line = jnp.concatenate(
+                [scales[n, 0:1, :] if q == order[0] else ones for q in range(first)], axis=1
+            )
+            lanes = lax.broadcasted_iota(jnp.int32, (slot, slot_weight.shape[3]), 1)
+            for e in range(local_experts):
+                chosen = table[0, n, pl.ds(e * slot, slot), :].astype(jnp.float32)
+                total = jnp.sum(chosen * line, axis=1, keepdims=True)
+                here = pl.ds(pl.multiple_of(n * slot, slot), slot)
+                slot_weight[0, e, here, :] = jnp.where(
+                    lanes < slot_weight.shape[3] // 2, slot_weight[0, e, here, :], total
+                )
+            return carry
+
+        lax.fori_loop(0, 4, fill, 0)
+
     def spread_rows(q):
         for k in range(2):
             send(
@@ -540,6 +581,10 @@
                 value = jnp.dot(
                     packed[e], up_now[side, :, cols], preferred_element_type=jnp.float32
                 )
+                if b == 0:
+                    middle = slot_weight.shape[3] // 2
+                    factor = slot_weight[b, e, :, middle : middle + 1]
+                    gate, value = gate * factor, value * factor
                 hidden[:, cols] = (gate / (1.0 + jnp.exp(-gate)) * value).astype(jnp.bfloat16)
                 return carry
 
@@ -660,14 +705,14 @@
     total = jnp.zeros((SUB, 1), jnp.float32)
     for k in range(4):
         if k == 3:
-            for step in steps:
+            for step in range(1, planes):
                 spread_corner(step)
         other_half(k)
         total = total + project_tile(order[0], places[k])
-    normalize_rows(order[0], total)
-    spread_rows(order[0])
+        spread_tile(order[0], places[k])
+    send_scales(total)
     make_tables()
-    for q in range(3, subs):
+    for q in range(2, subs):
         convolve(q)
     for at_q in range(1, first):
         sent_trade(order[at_q])
@@ -697,6 +742,7 @@
             near_of[k],
             tp,
         )
+    place_scales()
     run_experts(0, lambda: relay_rows(order[first]))
     combine(0, 3)
     send_first(0)
@@ -731,6 +777,7 @@
     left(proj.at[pl.ds(0, (planes - 1) * channels // 4)], corner_send.at[0])
     left(proj.at[pl.ds(0, (planes - 1) * channels)], core_send.at[0])
     left(early_resid, resid_send.at[0])
+    left(scales.at[pl.ds(1, 3)], scale_send.at[0])
     left(early_normed, normed_send.at[0])
     left(gathered.at[1, 3, pl.ds(half - early, early)], normed_send.at[1])
     for q in range(subs):
@@ -797,6 +844,7 @@
             pltpu.VMEM((2, 2, half, width), jnp.bfloat16),
             pltpu.VMEM((2, EARLY, width), jnp.bfloat16),
             pltpu.VMEM((2, EARLY, tp_count * channels), jnp.bfloat16),
+            pltpu.VMEM((4, 8, SUB), jnp.float32),
             dma((11,)),
             dma((3,)),
             dma((3,)),
@@ -826,6 +874,8 @@
             dma((1,)),
             dma((2,)),
             dma((2,)),
+            dma((1,)),
+            dma((1,)),
         ],
         compiler_params=pltpu.CompilerParams(
             collective_id=0, has_side_effects=True, vmem_limit_bytes=59944 * 1024

time: 167 us -> 164 us (0.982)
  Pallas kernels: 163 us -> 160 us
    pallas_call x1, Pallas kernels: 163 us -> 160 us  [front(): pl.pallas_call(functools.partial(front_kernel, tp_count), out_shape=[pltp...]
where the time goes in v4:
time: 164 us; the launch traced here: 161 us
  Pallas kernels  160 us (98%)
    pallas_call x1, Pallas kernels, front(): pl.pallas_call(functools.partial(front_kernel, tp_count), out_shape=[pltp...  160 us

profile of v4, /device:TPU:8, one launch (start us, length us, event | category | flops | bytes accessed | tf_op | source)
XLA Modules:
  0.0 161.2 jit_solution(15876816159931238853)
XLA Ops:
  0.0 159.7 %front.1 = (bf16[256,2048]{1,0:T(8,128)(2,1)S(1)}, bf16[256,2048]{1,0:T(8,128)(2,1)S(1)}) custom-call(bf16[128,4096]{1,0:T(8,128)(2,1)} %conv_in.1, bf16[128,4096]{1,0:T(8,128)(2,1)} %in_gate.1, bf16[128,4096]{1,0:T(8,128)(2,1)} %out_gate.1, s32[1,4096]{1,0:T(1,128)} %bitcast.6, f32[3,128]{1,0:T(4,128)} %bitcast.10, f32[1,128]{1,0:T(1,128)} %bitcast.11, ...), custom_call_target="tpu_custom_call" | custom-call | tf_op jit(solution)/shard_map/front/pallas_call | solution.py:810
  159.7 1.5 pad_maximum_fusion

commit v5 on v4

--- a/solution.py
+++ b/solution.py
@@ -96,6 +96,7 @@
     early_resid,
     early_normed,
     scales,
+    tails,
     local_sem,
     edge_send,
     edge_recv,
@@ -185,17 +186,14 @@
 
     after, before = (sp + 1) % 4, (sp + 3) % 4
     edge = pl.ds(0, SUB)
-    for at, (source, target) in enumerate(
-        ((conv_in, in_buf), (in_gate, gate_buf), (doc_ids, doc_buf))
-    ):
-        send(
-            source.at[:, pl.ds(tail, SUB)],
-            target.at[:, edge],
-            edge_send.at[at],
-            edge_recv.at[at],
-            after,
-            tp,
-        )
+    send(
+        doc_ids.at[:, pl.ds(tail, SUB)],
+        doc_buf.at[:, edge],
+        edge_send.at[0],
+        edge_recv.at[0],
+        after,
+        tp,
+    )
 
     eighth = width // 8
 
@@ -237,6 +235,10 @@
     for k in range(3):
         spread[k] = jnp.broadcast_to(taps[k : k + 1, :], (channels, channels)).T
     spread[3] = jnp.broadcast_to(gain[...], (channels, channels)).T
+    for at, source in enumerate((in_buf, gate_buf)):
+        last = source[:, pl.ds(tail + SUB, SUB)].astype(jnp.float32).T
+        tails[0, at] = last[SUB - 8 :].astype(jnp.bfloat16)
+    send(tails.at[0], tails.at[1], edge_send.at[1], edge_recv.at[1], after, tp)
     def piece(owner, q):
         base = pl.multiple_of(owner * rows + q * SUB, SUB)
         wide = pl.ds(base, 2 * SUB)
@@ -293,7 +295,7 @@
         arrive(region, slice_recv.at[step])
         for k in range(2):
             send(region, region, plane_send.at[0], plane_recv.at[k, step - 1], near_of[k], tp)
-        send(region, region, core_send.at[0], core_recv.at[0, step - 1], sp, tp ^ 1)
+        send(region, region, core_send.at[0], core_recv.at[0], sp, tp ^ 1)
 
     def spread_plane(step):
         for k in range(2):
@@ -301,21 +303,17 @@
             arrive(region, plane_recv.at[k, step - 1])
             part = proj.at[part_rows(step, k), columns(near_of[k], core)]
             send(part, part, corner_send.at[0], corner_recv.at[step - 1], near_of[1 - k], tp)
-            send(region, region, core_send.at[0], core_recv.at[1 + k, step - 1], sp, tp ^ 1)
+            send(region, region, core_send.at[0], core_recv.at[1 + k], sp, tp ^ 1)
 
     def spread_corner(step):
         region = proj.at[block_rows(step), columns(diagonal, core)]
         arrive(region, corner_recv.at[step - 1])
-        send(region, region, core_send.at[0], core_recv.at[3, step - 1], sp, tp ^ 1)
+        send(region, region, core_send.at[0], core_recv.at[3], sp, tp ^ 1)
 
     places = (sp, near_of[0], near_of[1], diagonal)
 
     def other_half(k):
-        for step in range(1, planes):
-            arrive(
-                proj.at[block_rows(step), columns(places[k], 1 - core)],
-                core_recv.at[k, step - 1],
-            )
+        arrive(proj.at[pl.ds(0, (planes - 1) * channels // 4)], core_recv.at[k])
 
     order = [1, 0, *range(2, subs)]
 
@@ -333,8 +331,12 @@
         spread_slice(step)
     left(proj.at[pl.ds(0, 2 * (planes - 1) * channels // 8)], slice_send.at[1])
     start_trade(order[0])
-    for k, target in enumerate((in_buf, gate_buf, doc_buf)):
-        arrive(target.at[:, edge], edge_recv.at[k])
+    arrive(doc_buf.at[:, edge], edge_recv.at[0])
+    arrive(tails.at[1], edge_recv.at[1])
+    for at, target in enumerate((in_buf, gate_buf)):
+        filler = jnp.zeros((SUB - 8, channels), jnp.float32)
+        last = jnp.concatenate([filler, tails[1, at].astype(jnp.float32)], axis=0)
+        target[:, edge] = last.T.astype(jnp.bfloat16)
     doc_buf[:, edge] = jnp.where(sp == 0, -1, doc_buf[:, edge])
     convolve(0)
     for step in range(1, planes):
@@ -645,12 +647,12 @@
                 partial.at[b, 1 + k, part_of[k]],
                 back.at[b, k, part_of[k]],
                 back_send.at[b],
-                straight_recv.at[b, k],
+                straight_recv.at[b],
                 near_of[k],
                 tp,
             )
 
-    strip = 16
+    strip = 32
 
     def merge(b):
         for k in range(2):
@@ -670,16 +672,15 @@
                 partial.at[b, 2 - k, part_of[k]],
                 back.at[b, 1 - k, part_of[k]],
                 back_send.at[b],
-                merged_recv.at[b, k],
+                merged_recv.at[b],
                 near_of[1 - k],
                 tp,
             )
 
     def finish(b):
+        arrive(back.at[b, 0], straight_recv.at[b])
+        arrive(back.at[b, 1], merged_recv.at[b])
         for k in range(2):
-            arrive(back.at[b, k, part_of[k]], straight_recv.at[b, k])
-        for k in range(2):
-            arrive(back.at[b, 1 - k, part_of[k]], merged_recv.at[b, k])
 
             def add(at, carry, k=k):
                 here = pl.ds(pl.multiple_of(k * (half // 2) + at * strip, strip), strip)
@@ -768,8 +769,8 @@
     finish(0)
     merge(1)
     finish(1)
-    for at, target in enumerate((in_buf, gate_buf, doc_buf)):
-        left(target.at[:, edge], edge_send.at[at])
+    left(doc_buf.at[:, edge], edge_send.at[0])
+    left(tails.at[0], edge_send.at[1])
     left(ids_out.at[pl.ds(1, 3)], list_send.at[0])
     left(weights_out.at[pl.ds(1, 3)], list_send.at[1])
     left(proj.at[my_rows], slice_send.at[0])
@@ -845,9 +846,10 @@
             pltpu.VMEM((2, EARLY, width), jnp.bfloat16),
             pltpu.VMEM((2, EARLY, tp_count * channels), jnp.bfloat16),
             pltpu.VMEM((4, 8, SUB), jnp.float32),
+            pltpu.VMEM((2, 2, 8, SUB), jnp.bfloat16),
             dma((11,)),
-            dma((3,)),
-            dma((3,)),
+            dma((2,)),
+            dma((2,)),
             dma((2,)),
             dma((2,)),
             dma((2,)),
@@ -857,7 +859,7 @@
             dma((1,)),
             dma((planes - 1,)),
             dma((1,)),
-            dma((4, planes - 1)),
+            dma((4,)),
             dma((subs,)),
             dma((subs,)),
             dma((subs,)),
@@ -868,8 +870,8 @@
             dma((2,)),
             dma((2, 2)),
             dma((2,)),
-            dma((2, 2)),
-            dma((2, 2)),
+            dma((2,)),
+            dma((2,)),
             dma((1,)),
             dma((1,)),
             dma((2,)),

time: 164 us -> 164 us (level)
  no operation moved by 1% of the time
where the time goes in v5:
time: 164 us; the launch traced here: 161 us
  Pallas kernels  159 us (97%)
    pallas_call x1, Pallas kernels, front(): pl.pallas_call(functools.partial(front_kernel, tp_count), out_shape=[pltp...  159 us

profile of v5, /device:TPU:8, one launch (start us, length us, event | category | flops | bytes accessed | tf_op | source)
XLA Modules:
  0.0 160.8 jit_solution(8454566025635466733)
XLA Ops:
  0.0 159.3 %front.1 = (bf16[256,2048]{1,0:T(8,128)(2,1)S(1)}, bf16[256,2048]{1,0:T(8,128)(2,1)S(1)}) custom-call(bf16[128,4096]{1,0:T(8,128)(2,1)} %conv_in.1, bf16[128,4096]{1,0:T(8,128)(2,1)} %in_gate.1, bf16[128,4096]{1,0:T(8,128)(2,1)} %out_gate.1, s32[1,4096]{1,0:T(1,128)} %bitcast.6, f32[3,128]{1,0:T(4,128)} %bitcast.10, f32[1,128]{1,0:T(1,128)} %bitcast.11, ...), custom_call_target="tpu_custom_call" | custom-call | tf_op jit(solution)/shard_map/front/pallas_call | solution.py:811
  159.3 1.5 pad_maximum_fusion

commit v6 on v5

--- a/solution.py
+++ b/solution.py
@@ -763,9 +763,8 @@
     send_first(1)
     combine(1, 1)
     combine(1, 2)
+    send_straight(1)
     combine(1, 0)
-    left(partial.at[1, 3], first_send.at[1])
-    send_straight(1)
     finish(0)
     merge(1)
     finish(1)
@@ -789,6 +788,7 @@
         if q != order[0]:
             left(near_region(0, q), far_send.at[q])
     left(partial.at[0, 3], first_send.at[0])
+    left(partial.at[1, 3], first_send.at[1])
     for b in range(2):
         left(back.at[b], back_send.at[b])
 

time: 164 us -> 163 us (level)
  no operation moved by 1% of the time
where the time goes in v6:
time: 163 us; the launch traced here: 160 us
  Pallas kernels  159 us (98%)
    pallas_call x1, Pallas kernels, front(): pl.pallas_call(functools.partial(front_kernel, tp_count), out_shape=[pltp...  159 us

profile of v6, /device:TPU:8, one launch (start us, length us, event | category | flops | bytes accessed | tf_op | source)
XLA Modules:
  0.0 160.1 jit_solution(2422166786747977910)
XLA Ops:
  0.0 158.6 %front.1 = (bf16[256,2048]{1,0:T(8,128)(2,1)S(1)}, bf16[256,2048]{1,0:T(8,128)(2,1)S(1)}) custom-call(bf16[128,4096]{1,0:T(8,128)(2,1)} %conv_in.1, bf16[128,4096]{1,0:T(8,128)(2,1)} %in_gate.1, bf16[128,4096]{1,0:T(8,128)(2,1)} %out_gate.1, s32[1,4096]{1,0:T(1,128)} %bitcast.6, f32[3,128]{1,0:T(4,128)} %bitcast.10, f32[1,128]{1,0:T(1,128)} %bitcast.11, ...), custom_call_target="tpu_custom_call" | custom-call | tf_op jit(solution)/shard_map/front/pallas_call | solution.py:811
  158.6 1.5 pad_maximum_fusion
